TPU v7x, 256 devices: a whole 4x4x8 slice. The times are simulated.
256 devices in a mesh: rep: 2 (over z_hi), fs: 16 (over z_lo, y), tp: 8 (over x, core).
Axes of the slice: x: 4, y: 4, z: 8 (z_hi: 2, z_lo: 4; z = z_hi * 4 + z_lo), core: 2. Of those that a mesh axis runs over, the one named last changes fastest.
Arguments:
- stream: bfloat16 [16384, 2048], P(('rep', 'fs'), 'tp'), parts along dimension 0, may hold values from -6 to 6
- in_weight: bfloat16 [2048, 1024], P('fs', 'tp'), may hold values from -0.125 to 0.125
- pool_weight: bfloat16 [8, 128, 128], P('tp'), may hold values from -0.5 to 0.5
- pool_scale: bfloat16 [1024], P('tp'), may hold values from 0.099609375 to 1.8984375
- out_weight: bfloat16 [1024, 2048], P('tp', 'fs'), may hold values from -0.1875 to 0.1875
- mix_gain: bfloat16 [2048], replicated, may hold values from 0.099609375 to 1.8984375
- ffn_gain: bfloat16 [2048], replicated, may hold values from 0.099609375 to 1.8984375
- gate_weight: bfloat16 [2048, 5632], P('fs', 'tp'), may hold values from -0.125 to 0.125
- up_weight: bfloat16 [2048, 5632], P('fs', 'tp'), may hold values from -0.125 to 0.125
- down_weight: bfloat16 [5632, 2048], P('tp', 'fs'), may hold values from -0.078125 to 0.078125
Outputs:
- result: bfloat16 [16384, 2048], P(('rep', 'fs'), 'tp'), parts along dimension 0
There are 2 independent parts, one for each index of `rep`. A program takes and returns all parts, laid end to end along the dimension named above; an argument that names none is the same for every part. Nothing has to cross between parts.
All inputs are finite; a program needn't handle non-finite values.
Results may differ from a plain program's by a relative error of at most 0.015.
Values may be sent and summed in bfloat16 or wider, within the bound.
A program may use at most 64 MiB of HBM per device.

v0:
```python
import jax
import jax.numpy as jnp
from jax import lax
from jax.sharding import Mesh
from jax.sharding import PartitionSpec as P

GROUPS = 8
SEQ = 128
FS = ("fs_0", "fs_1")
REP_FS = ("rep", "fs_0", "fs_1")


epsilon = 1e-06


def in_order(parts, dim):
    lengths = list(parts.shape[1:])
    lengths[dim] *= parts.shape[0]
    return jnp.moveaxis(parts, 0, dim).reshape(lengths)


def sent_to_all(array, axis):
    length = lax.axis_size(axis)
    return lax.all_to_all(
        jnp.broadcast_to(array[None], (length, *array.shape)), axis, 0, 0, tiled=True
    )


def gather_directly(array, axis, dim):
    return in_order(sent_to_all(array, axis), dim)


def split_up(array, dim, length):
    lengths = array.shape
    parts = array.reshape(*lengths[:dim], length, lengths[dim] // length, *lengths[dim + 1 :])
    return jnp.moveaxis(parts, dim, 0)


def sum_at_owner(array, axis, dim):
    parts = split_up(array, dim, lax.axis_size(axis))
    arrived = lax.all_to_all(parts, axis, split_axis=0, concat_axis=0, tiled=True)
    return arrived.astype(jnp.float32).sum(axis=0)


def sent_together(arrays, axis, dim, along):
    ends, at = ([], 0)
    for a in arrays[:-1]:
        at += a.shape[along]
        ends.append(at)
    both = jnp.concatenate(arrays, axis=along)
    return tuple(jnp.split(lax.all_gather(both, axis, axis=dim, tiled=True), ends, axis=along))


def all_blocks(array, axes, sequence):
    parts = array
    for k in sequence:
        parts = lax.all_gather(parts, axes[k])
    done = sequence[::-1]
    back = [done.index(k) for k in range(len(axes))]
    parts = parts.transpose(*back, *range(len(axes), parts.ndim))
    return parts.reshape(-1, *array.shape)


def gather_axes(array, axes, sequence, dim):
    return in_order(all_blocks(array, axes, sequence), dim)


def root_norm(values, gain_vec):
    widened = values.astype(jnp.float32)
    scaled = widened * lax.rsqrt(jnp.mean(widened * widened, axis=-1, keepdims=True) + epsilon)
    return (scaled * gain_vec.astype(jnp.float32)).astype(jnp.bfloat16)


def window_tables(first_group, group_count, seq_len, total_groups):
    group_ids = first_group + jnp.arange(group_count, dtype=jnp.int32)
    reaches = jnp.left_shift(jnp.int32(2), 4 * group_ids // total_groups)
    query_pos = jnp.arange(seq_len, dtype=jnp.int32)[:, None]
    earlier = jnp.arange(seq_len, dtype=jnp.int32)[None, :]
    inside = (earlier <= query_pos)[None] & (
        earlier[None] > query_pos[None] - reaches[:, None, None]
    )
    counts = jnp.minimum(query_pos[:, 0][None, :] + 1, reaches[:, None]).astype(jnp.float32)
    return (inside, counts)


def full_rows(values):
    return gather_directly(values, "tp", 1)


def on_device(
    stream,
    in_weight,
    pool_weight,
    pool_scale,
    out_weight,
    mix_gain,
    ffn_gain,
    gate_weight,
    up_weight,
    down_weight,
):
    normed = root_norm(full_rows(stream), mix_gain)
    tokens = normed.shape[0]
    local_groups = pool_weight.shape[0]
    group_dim = pool_weight.shape[1]
    token_cols = normed
    pooled_in = jnp.dot(
        token_cols, gather_directly(in_weight, FS, 0), preferred_element_type=jnp.float32
    ).astype(jnp.bfloat16)
    first_group = lax.axis_index("tp") * local_groups
    inside, counts = window_tables(first_group, local_groups, SEQ, GROUPS)
    grouped = pooled_in.reshape(tokens // SEQ, SEQ, local_groups, group_dim)
    window_sums = jnp.einsum(
        "gts,nsgc->ntgc", inside.astype(jnp.bfloat16), grouped, preferred_element_type=jnp.float32
    )
    contrast = (window_sums / counts.T[None, :, :, None] - grouped.astype(jnp.float32)).astype(
        jnp.bfloat16
    )
    mixed_out = jnp.einsum(
        "ntgc,gcd->ntgd", contrast, pool_weight, preferred_element_type=jnp.float32
    )
    group_out = (
        mixed_out.reshape(tokens, local_groups * group_dim) * pool_scale.astype(jnp.float32)
    ).astype(jnp.bfloat16)
    partials = jnp.dot(
        group_out, gather_directly(out_weight, FS, 1), preferred_element_type=jnp.float32
    )
    mixer_sum = sum_at_owner(partials.astype(jnp.bfloat16), "tp", 1)
    middle = (stream.astype(jnp.float32) + mixer_sum).astype(jnp.bfloat16)
    normed_ffn = root_norm(full_rows(middle), ffn_gain)
    pieces = sent_together((gate_weight, up_weight), FS, 0, 1)
    token_cols = normed_ffn
    gate_acts = jnp.dot(token_cols, pieces[0], preferred_element_type=jnp.float32)
    up_acts = jnp.dot(token_cols, pieces[1], preferred_element_type=jnp.float32)
    hidden = (jax.nn.silu(gate_acts) * up_acts).astype(jnp.bfloat16)
    ffn_partials = jnp.dot(
        hidden, gather_axes(down_weight, FS, (0, 1), 1), preferred_element_type=jnp.float32
    )
    ffn_sum = sum_at_owner(ffn_partials.astype(jnp.bfloat16), "tp", 1)
    return (middle.astype(jnp.float32) + ffn_sum).astype(jnp.bfloat16)


def solution(mesh):
    finer = Mesh(
        mesh.devices.reshape(mesh.shape["rep"], 4, 4, mesh.shape["tp"]),
        ("rep", "fs_0", "fs_1", "tp"),
    )
    return jax.shard_map(
        on_device,
        mesh=finer,
        in_specs=(
            P(REP_FS, "tp"),
            P(FS, "tp"),
            P("tp", None, None),
            P("tp"),
            P("tp", FS),
            P(),
            P(),
            P(FS, "tp"),
            P(FS, "tp"),
            P("tp", FS),
        ),
        out_specs=P(REP_FS, "tp"),
        check_vma=False,
    )
```

profile of v0, /device:TPU:1, one launch (start us, length us, event | category | flops | bytes accessed | tf_op | source)
XLA Modules:
  0.0 237.0 jit_solution(7466743238574650469)
XLA Ops:
  6.5 0.0 copy-start
  6.5 0.0 copy-start.2
  6.5 0.0 all-gather.7.cloned.1.call-start
  6.5 19.2 %all-gather = bf16[2816,128]{1,0:T(8,128)(2,1)} all-gather(bf16[704,128]{1,0:T(8,128)(2,1)} %param.19), channel_id=2, replica_groups=mesh['rep'=2,'fs_0'=4,'fs_1'=4,'tp'=8] {'fs_0'}, dimensions={0}, use_global_device_ids=true | all-gather | bytes 901120 | tf_op jit(solution)/shard_map/all_gather | solution.py:57
  25.8 0.0 all-gather.7.cloned.1.call-update
  25.8 0.0 all-gather.5.cloned.1.call-start
  25.8 1.8 pad_maximum_fusion
  27.6 0.0 all-gather.5.cloned.1.call-update
  27.6 0.0 copy-done.2
  27.6 0.1 copy.29
  27.8 0.2 broadcast_in_dim.8
  28.0 0.0 copy-start.3
  28.0 0.0 copy-start.7
  28.0 0.0 copy-start.5
  28.0 0.0 copy-start.4
  28.0 33.6 %all_to_all.30 = bf16[8,512,256]{1,2,0:T(8,128)(2,1)S(1)} all-to-all(bf16[8,512,256]{1,2,0:T(8,128)(2,1)S(1)} %broadcast_in_dim.8), channel_id=1, replica_groups=mesh['rep'=2,'fs_0'=4,'fs_1'=4,'tp'=8] {'tp'}, dimensions={0} | all-to-all | bytes 4194304 | tf_op jit(solution)/shard_map/all_to_all | solution.py:24
  61.6 0.0 copy-done.3
  61.6 0.9 broadcast_in_dim.9
  62.5 5.7 %all-to-all-start.1 = ((bf16[16,128,128]{2,1,0:T(8,128)(2,1)}), bf16[16,128,128]{2,1,0:T(8,128)(2,1)S(1)}, u32[]{:S(2)}, u32[]{:S(2)}) async-start(bf16[16,128,128]{2,1,0:T(8,128)(2,1)} %broadcast_in_dim.9), calls=%async_computation.1 | async-start | bytes 1048576 | tf_op jit(solution)/shard_map/all_to_all | solution.py:24
  68.2 0.0 copy-done.7
  68.3 0.0 copy-done.5
  68.3 0.0 copy-done.4
  68.3 0.1 copy.33
  68.5 0.5 fusion
  69.0 12.9 %all-to-all-done.1 = bf16[16,128,128]{2,1,0:T(8,128)(2,1)S(1)} async-done(((bf16[16,128,128]{2,1,0:T(8,128)(2,1)}), bf16[16,128,128]{2,1,0:T(8,128)(2,1)S(1)}, u32[]{:S(2)}, u32[]{:S(2)}) %all-to-all-start.1) | async-done | bytes 524320 | tf_op jit(solution)/shard_map/all_to_all | solution.py:24
  81.8 0.9 broadcast_in_dim.10
  82.7 5.5 %all-to-all-start.2 = ((bf16[16,128,128]{1,2,0:T(8,128)(2,1)}), bf16[16,128,128]{1,2,0:T(8,128)(2,1)S(1)}, u32[]{:S(2)}, u32[]{:S(2)}) async-start(bf16[16,128,128]{1,2,0:T(8,128)(2,1)} %broadcast_in_dim.10), calls=%async_computation.2 | async-start | bytes 1048576 | tf_op jit(solution)/shard_map/all_to_all | solution.py:24
  88.2 0.5 fusion.2
  88.7 0.8 convolution_convert_fusion.2
  89.5 0.1 copy.31
  89.6 0.0 copy-done
  89.6 0.5 fusion.18
  90.1 24.2 %all-to-all-done.2 = bf16[16,128,128]{1,2,0:T(8,128)(2,1)S(1)} async-done(((bf16[16,128,128]{1,2,0:T(8,128)(2,1)}), bf16[16,128,128]{1,2,0:T(8,128)(2,1)S(1)}, u32[]{:S(2)}, u32[]{:S(2)}) %all-to-all-start.2) | async-done | bytes 524320 | tf_op jit(solution)/shard_map/all_to_all | solution.py:24
  114.3 0.7 convolution_convert_fusion
  115.0 0.1 copy.51
  115.2 34.5 %all_to_all.31 = bf16[8,512,256]{2,1,0:T(8,128)(2,1)S(1)} all-to-all(bf16[8,512,256]{2,1,0:T(8,128)(2,1)S(1)} %bitcast.101), channel_id=1, replica_groups=mesh['rep'=2,'fs_0'=4,'fs_1'=4,'tp'=8] {'tp'}, dimensions={0} | all-to-all | bytes 4194304 | tf_op jit(solution)/shard_map/all_to_all | solution.py:41
  149.7 0.3 convert_reduce_fusion.1
  150.0 0.1 add_convert_fusion.1
  150.0 0.1 copy.35
  150.2 1.6 broadcast_in_dim.11
  151.8 0.0 copy-start.6
  151.8 4.3 %all-to-all-start.4 = ((bf16[8,512,256]{1,2,0:T(8,128)(2,1)}), bf16[8,512,256]{1,2,0:T(8,128)(2,1)S(1)}, u32[]{:S(2)}, u32[]{:S(2)}) async-start(bf16[8,512,256]{1,2,0:T(8,128)(2,1)} %broadcast_in_dim.11), calls=%async_computation.4 | async-start | bytes 4194304 | tf_op jit(solution)/shard_map/all_to_all | solution.py:24
  156.1 0.0 copy-done.6
  156.1 0.0 all-gather.7.cloned.1.call-done
  156.1 3.7 %copy.36 = bf16[4,4,704,128]{3,2,1,0:T(8,128)(2,1)} copy(bf16[4,4,704,128]{3,2,0,1:T(8,128)(2,1)} %bitcast.103) | data formatting | bytes 5767168 | tf_op jit(solution)/shard_map/transpose | solution.py:60
  159.8 22.5 %all-to-all-done.4 = bf16[8,512,256]{1,2,0:T(8,128)(2,1)S(1)} async-done(((bf16[8,512,256]{1,2,0:T(8,128)(2,1)}), bf16[8,512,256]{1,2,0:T(8,128)(2,1)S(1)}, u32[]{:S(2)}, u32[]{:S(2)}) %all-to-all-start.4) | async-done | bytes 2097184 | tf_op jit(solution)/shard_map/all_to_all | solution.py:24
  182.3 0.5 multiply_reduce_fusion
  182.8 1.9 fusion.4
  184.7 0.0 copy-start.1
  184.7 0.0 all-gather.5.cloned.1.call-done
  184.7 5.4 %fusion.9 = f32[512,704]{0,1:T(8,128)} fusion(bf16[512,2048]{0,1:T(8,128)(2,1)} %fusion.4, bf16[2048,1408]{0,1:T(8,128)(2,1)} %all-gather.5.cloned.1.call-done), kind=kOutput, calls=%fused_computation.17 | convolution fusion | flops 1476395008 | bytes 6422528 | tf_op jit(solution)/shard_map/dot_general | solution.py:133
  190.1 0.0 copy-done.1
  190.1 7.6 %convolution_convert_fusion.1 = bf16[512,2048]{1,0:T(8,128)(2,1)} fusion(bf16[16,88,8,128]{3,2,1,0:T(8,128)(2,1)S(1)} %bitcast.104, bf16[512,2048]{0,1:T(8,128)(2,1)} %fusion.4, bf16[2048,1408]{0,1:T(8,128)(2,1)} %all-gather.5.cloned.1.call-done, f32[512,704]{0,1:T(8,128)} %fusion.9), kind=kOutput, calls=%fused_computation.12 | convolution fusion | flops 2956001280 | bytes 11403264 | tf_op jit(solution)/shard_map/dot_general | solution.py:136
  197.8 1.7 copy.50
  199.5 29.6 %all_to_all.32 = bf16[8,512,256]{2,1,0:T(8,128)(2,1)S(1)} all-to-all(bf16[8,512,256]{2,1,0:T(8,128)(2,1)S(1)} %bitcast.102), channel_id=1, replica_groups=mesh['rep'=2,'fs_0'=4,'fs_1'=4,'tp'=8] {'tp'}, dimensions={0} | all-to-all | bytes 4194304 | tf_op jit(solution)/shard_map/all_to_all | solution.py:41
  229.1 0.3 convert_reduce_fusion
  229.4 0.8 add_convert_fusion
  (6 shorter events, 0.0 us)
Async XLA Ops:
  6.5 83.1 %copy-start = (bf16[1,128,128]{2,1,0:T(8,128)(2,1)S(1)}, bf16[1,128,128]{2,1,0:T(8,128)(2,1)}, u32[]{:S(2)}) copy-start(bf16[1,128,128]{2,1,0:T(8,128)(2,1)} %param.12) | copy-start | bytes 98308
  6.5 21.1 %copy-start.2 = (bf16[512,256]{1,0:T(8,128)(2,1)S(1)}, bf16[512,256]{1,0:T(8,128)(2,1)}, u32[]{:S(2)}) copy-start(bf16[512,256]{1,0:T(8,128)(2,1)} %param.10) | copy-start | bytes 786436
  6.5 149.6 %all-gather.7.cloned.1.call-start = ((), (), s32[]{:S(2)}) async-start(), calls=%async_computation.7 | async-start | bytes 3604480 | tf_op jit(solution)/shard_map/all_gather | solution.py:57
  25.8 158.9 %all-gather.5.cloned.1.call-start = ((), (), s32[]{:S(2)}) async-start(), calls=%async_computation.6 | async-start | bytes 6127616 | tf_op jit(solution)/shard_map/all_gather | solution.py:51
  28.0 33.7 %copy-start.3 = (bf16[128,128]{1,0:T(8,128)(2,1)S(1)}, bf16[128,128]{1,0:T(8,128)(2,1)}, u32[]{:S(2)}) copy-start(bf16[128,128]{1,0:T(8,128)(2,1)} %param.11) | copy-start | bytes 98308
  28.0 40.3 %copy-start.7 = (bf16[128]{0:T(256)(128)(2,1)S(1)}, bf16[128]{0:T(256)(128)(2,1)}, u32[]{:S(2)}) copy-start(bf16[128]{0:T(256)(128)(2,1)} %param.13) | copy-start | bytes 772
  28.0 40.3 %copy-start.5 = (bf16[2048]{0:T(1024)(128)(2,1)S(1)}, bf16[2048]{0:T(1024)(128)(2,1)}, u32[]{:S(2)}) copy-start(bf16[2048]{0:T(1024)(128)(2,1)} %param.15) | copy-start | bytes 12292
  28.0 40.3 %copy-start.4 = (bf16[128,128]{1,0:T(8,128)(2,1)S(1)}, bf16[128,128]{1,0:T(8,128)(2,1)}, u32[]{:S(2)}) copy-start(bf16[128,128]{1,0:T(8,128)(2,1)} %param.14) | copy-start | bytes 98308
  62.5 19.3 %all-to-all-start.1 = ((bf16[16,128,128]{2,1,0:T(8,128)(2,1)}), bf16[16,128,128]{2,1,0:T(8,128)(2,1)S(1)}, u32[]{:S(2)}, u32[]{:S(2)}) async-start(bf16[16,128,128]{2,1,0:T(8,128)(2,1)} %broadcast_in_dim.9), calls=%async_computation.1 | async-start | bytes 1048576 | tf_op jit(solution)/shard_map/all_to_all | solution.py:24
  82.7 31.6 %all-to-all-start.2 = ((bf16[16,128,128]{1,2,0:T(8,128)(2,1)}), bf16[16,128,128]{1,2,0:T(8,128)(2,1)S(1)}, u32[]{:S(2)}, u32[]{:S(2)}) async-start(bf16[16,128,128]{1,2,0:T(8,128)(2,1)} %broadcast_in_dim.10), calls=%async_computation.2 | async-start | bytes 1048576 | tf_op jit(solution)/shard_map/all_to_all | solution.py:24
  151.8 4.3 %copy-start.6 = (bf16[2048]{0:T(1024)(128)(2,1)S(1)}, bf16[2048]{0:T(1024)(128)(2,1)}, u32[]{:S(2)}) copy-start(bf16[2048]{0:T(1024)(128)(2,1)} %param.16) | copy-start | bytes 12292
  151.8 30.5 %all-to-all-start.4 = ((bf16[8,512,256]{1,2,0:T(8,128)(2,1)}), bf16[8,512,256]{1,2,0:T(8,128)(2,1)S(1)}, u32[]{:S(2)}, u32[]{:S(2)}) async-start(bf16[8,512,256]{1,2,0:T(8,128)(2,1)} %broadcast_in_dim.11), calls=%async_computation.4 | async-start | bytes 4194304 | tf_op jit(solution)/shard_map/all_to_all | solution.py:24
  184.7 5.4 %copy-start.1 = (bf16[4,4,704,128]{3,2,1,0:T(8,128)(2,1)S(1)}, bf16[4,4,704,128]{3,2,1,0:T(8,128)(2,1)}, u32[]{:S(2)}) copy-start(bf16[4,4,704,128]{3,2,1,0:T(8,128)(2,1)} %copy.36) | copy-start | bytes 8650756
Sparse Core Ops, SparseCore 0:
  25.9 42.4 all-gather.6
  70.1 102.5 all-gather.4
where the time goes:
time: 241 us; the launch traced here: 237 us
  blocking collectives  117 us (49%)
  waiting for transfers between devices  59.7 us (25%)
  starting transfers between devices  15.5 us (6%)
  matrix products  15 us (6%)
  between operations  13.7 us (6%)
  local copies, waits for them, and re-layouts  9.63 us (4%)
  other arithmetic  6.62 us (3%)
    all_to_all x2, blocking collectives, sum_at_owner(): lax.all_to_all(parts, axis, split_axis=0, concat_axis=0, tiled=True)  64.1 us
    all_to_all x3, waiting for transfers between devices, sent_to_all(): lax.all_to_all(jnp.broadcast_to(array[None], (length, *array.shape)), axi...  59.6 us
    all_to_all x1, blocking collectives, sent_to_all(): lax.all_to_all(jnp.broadcast_to(array[None], (length, *array.shape)), axi...  33.6 us
    all_gather x1, blocking collectives, all_blocks(): parts = lax.all_gather(parts, axes[k])  19.2 us
    all_to_all x3, starting transfers between devices, sent_to_all(): lax.all_to_all(jnp.broadcast_to(array[None], (length, *array.shape)), axi...  15.5 us
    dot_general x1, matrix products, on_device(): jnp.dot(hidden, gather_axes(down_weight, FS, (0, 1), 1), preferred_elemen...  7.65 us
    dot_general x1, matrix products, on_device(): jnp.dot(token_cols, pieces[0], preferred_element_type=jnp.float32)  5.41 us
  transfers between devices with their start and end apart: 5, of which 3 were waited for; matrix products, arithmetic and copies ran while one was open for 6% of the time, Pallas kernels for 0%

commit v1 on v0

v1 whole, which is shorter than its diff:
```python
import jax
import jax.numpy as jnp
from jax import lax
from jax.experimental import pallas as pl
from jax.experimental.pallas import tpu as pltpu
from jax.sharding import Mesh
from jax.sharding import PartitionSpec as P

SEQ = 128
RING = 4
EPS = 1e-06
F32, BF16 = jnp.float32, jnp.bfloat16


class Place:
    def __init__(self):
        self.rep, self.z, self.y = (lax.axis_index(a) for a in ("rep", "fs_0", "fs_1"))
        self.x, self.core = lax.axis_index("x"), lax.axis_index("core")

    def to(self, axis, step):
        if axis == "core":
            return {"core": 1 - self.core}
        if axis == "z":
            deep = (self.rep * RING + self.z + step + 2 * RING) % (2 * RING)
            return {"rep": deep // RING, "fs_0": deep % RING}
        index = {"x": self.x, "y": self.y}[axis]
        return {{"x": "x", "y": "fs_1"}[axis]: (index + step + RING) % RING}


class Sends:
    def __init__(self, send_sems, recv_sems):
        self.send_sems, self.recv_sems, self.open = send_sems, recv_sems, []

    def send(self, k, src, dst, device):
        copy = pltpu.make_async_remote_copy(
            src_ref=src,
            dst_ref=dst,
            send_sem=self.send_sems.at[k],
            recv_sem=self.recv_sems.at[k],
            device_id=device,
            device_id_type=pl.DeviceIdType.MESH,
        )
        copy.start()
        self.open.append(copy)

    def arrived(self, k, ref):
        pltpu.make_async_copy(ref, ref, self.recv_sems.at[k]).wait()

    def drain(self):
        for copy in self.open:
            copy.wait_send()


class Gather:
    def __init__(self, place, buf, send_sems, recv_sems):
        self.place, self.buf = place, buf
        self.net = Sends(send_sems, recv_sems)
        half = buf.shape[2] // 2
        self.flows = (("y", "z", 0, half, 0), ("z", "y", half, half, 10))

    def block(self, axis, step, first, rows):
        z, y = self.place.z, self.place.y
        z, y = ((z + step) % RING, y) if axis == "z" else (z, (y + step) % RING)
        return self.buf.at[z, y, pl.ds(first, rows), :]

    def plane(self, axis, step, side, first, rows):
        two = pl.ds(2 * side, 2)
        if axis == "z":
            return self.buf.at[(self.place.z + step) % RING, two, pl.ds(first, rows), :]
        return self.buf.at[two, (self.place.y + step) % RING, pl.ds(first, rows), :]

    def p1_own(self):
        for axis, _, first, rows, k in self.flows:
            own = self.block(axis, 0, first, rows)
            self.net.send(k, own, own, self.place.to(axis, 1))
            self.net.send(k + 1, own, own, self.place.to(axis, -1))

    def p1_forward(self):
        for axis, _, first, rows, k in self.flows:
            half = rows // 2
            self.net.arrived(k, self.block(axis, 3, first, rows))
            low = self.block(axis, 3, first, half)
            self.net.send(k + 2, low, low, self.place.to(axis, 1))
            self.net.arrived(k + 1, self.block(axis, 1, first, rows))
            high = self.block(axis, 1, first + half, half)
            self.net.send(k + 3, high, high, self.place.to(axis, -1))

    def p2_own(self):
        for before, axis, first, rows, k in self.flows:
            half = rows // 2
            self.net.arrived(k + 2, self.block(before, 2, first, half))
            self.net.arrived(k + 3, self.block(before, 2, first + half, half))
            low, high = (self.plane(axis, 0, side, first, rows) for side in (0, 1))
            self.net.send(k + 4, low, low, self.place.to(axis, 1))
            self.net.send(k + 7, high, high, self.place.to(axis, -1))
            self.net.send(k + 5, high, high, self.place.to(axis, 1))
            self.net.send(k + 6, low, low, self.place.to(axis, -1))

    def p2_forward(self):
        for _, axis, first, rows, k in self.flows:
            low, high = self.plane(axis, 3, 0, first, rows), self.plane(axis, 1, 1, first, rows)
            self.net.arrived(k + 4, low)
            self.net.send(k + 8, low, low, self.place.to(axis, 1))
            self.net.arrived(k + 7, high)
            self.net.send(k + 9, high, high, self.place.to(axis, -1))

    def finish(self):
        for _, axis, first, rows, k in self.flows:
            self.net.arrived(k + 5, self.plane(axis, 3, 1, first, rows))
            self.net.arrived(k + 6, self.plane(axis, 1, 0, first, rows))
            self.net.arrived(k + 8, self.plane(axis, 2, 0, first, rows))
            self.net.arrived(k + 9, self.plane(axis, 2, 1, first, rows))


class Spread:
    def __init__(self, place, buf, send_sems, recv_sems):
        self.place, self.buf = place, buf
        self.net = Sends(send_sems, recv_sems)
        self.half = buf.shape[1] // 2

    def index(self, step, other=False):
        core = 1 - self.place.core if other else self.place.core
        return 2 * ((self.place.x + step) % RING) + core

    def part(self, step, side):
        return self.buf.at[self.index(step), pl.ds(side * self.half, self.half), :]

    def to_core(self, k, step):
        block = self.buf.at[self.index(step)]
        self.net.send(k, block, block, self.place.to("core", 0))

    def start(self):
        up, down = self.place.to("x", 1), self.place.to("x", -1)
        low, high = self.part(0, 0), self.part(0, 1)
        self.net.send(0, low, low, up)
        self.net.send(2, high, high, down)
        self.net.send(1, high, high, up)
        self.net.send(3, low, low, down)
        self.to_core(6, 0)

    def forward(self):
        low, high = self.part(3, 0), self.part(1, 1)
        self.net.arrived(0, low)
        self.net.send(4, low, low, self.place.to("x", 1))
        self.net.arrived(2, high)
        self.net.send(5, high, high, self.place.to("x", -1))

    def near(self):
        self.net.arrived(1, self.part(3, 1))
        self.to_core(7, 3)
        self.net.arrived(3, self.part(1, 0))
        self.to_core(8, 1)

    def far(self):
        self.net.arrived(4, self.part(2, 0))
        self.net.arrived(5, self.part(2, 1))
        self.to_core(9, 2)

    def from_core(self, k, step):
        self.net.arrived(k, self.buf.at[self.index(step, other=True)])


def kernel(
    stream, w_in, pool_w, pool_s, w_out, mix_gain, ffn_gain, w_gate, w_up, w_down, out,
    mixer, pair_a, pair_b, down, blocks_a, blocks_b, scaled, squares, rates, group_out, hidden,
    pair_out, pair_in, sums, last, combined, landed, gs, gr, xs, xr,
):
    place = Place()
    x, core, y, z = place.x, place.core, place.y, place.z
    mine = 2 * x + core
    tokens = stream.shape[0]
    half = tokens // 2

    barrier = pltpu.get_barrier_semaphore()
    neighbours = [place.to(a, s) for a in "xyz" for s in (1, -1)] + [place.to("core", 0)]
    for device in neighbours:
        pl.semaphore_signal(barrier, inc=1, device_id=device, device_id_type=pl.DeviceIdType.MESH)

    mixer[z, y, 0:128, :] = w_in[...]
    mixer[z, y, 128:256, :] = w_out[...]
    blocks_a[mine] = stream[...]
    for tile in range(5):
        buf, at = (pair_a, tile) if tile < 3 else (pair_b, tile - 3)
        lanes = slice(128 * tile, 128 * tile + 128)
        buf[z, y, :, 256 * at : 256 * at + 128] = w_gate[:, lanes]
        buf[z, y, :, 256 * at + 128 : 256 * at + 256] = w_up[:, lanes]
    pair_b[z, y, :, 512:640] = jnp.concatenate([w_gate[:, 640:704], w_up[:, 640:704]], axis=1)
    down[z, y] = w_down[...]

    pl.semaphore_wait(barrier, len(neighbours))

    gathers = [
        Gather(place, buf, gs.at[i], gr.at[i]) for i, buf in enumerate((mixer, pair_a, pair_b, down))
    ]
    g_mix, g_a, g_b, g_down = gathers
    s_in = Spread(place, blocks_a, xs.at[0], xr.at[0])
    s_mid = Spread(place, blocks_b, xs.at[1], xr.at[1])

    def take(buf, gain_ref, index, first=False):
        lanes = pl.ds(pl.multiple_of(index * 256, 256), 256)
        gain = gain_ref[:, lanes].astype(F32)

        def some(i, carry):
            rows = pl.ds(pl.multiple_of(i * 64, 64), 64)
            value = buf[index, rows, :].astype(F32)
            scaled[rows, lanes] = (value * gain).astype(BF16)
            square = value * value
            square = square[:, :128] + square[:, 128:]
            squares[rows, :] = square if first else squares[rows, :] + square
            return carry

        lax.fori_loop(0, tokens // 64, some, 0)

    def row_rates():
        total = jnp.sum(squares[...], axis=1, keepdims=True)
        rates[...] = jnp.broadcast_to(lax.rsqrt(total * (1.0 / 2048.0) + EPS), (tokens, 128))

    def rows_of(side):
        return pl.ds(side * half, half)

    class Summed:
        def __init__(self, which):
            self.net = Sends(xs.at[which], xr.at[which])
            self.out, self.into = pair_out.at[which], pair_in.at[which]
            self.sums, self.last = sums.at[which], last
            self.combined, self.landed = combined.at[which], landed.at[which]

        def pair(self, product):
            for j, step in enumerate((2, 1, 3, 0)):
                for side in (0, 1):
                    self.out[j, rows_of(side), :] = product((x + step) % RING, 1 - core, side).astype(BF16)
                self.net.send(10 + j, self.out.at[j], self.into.at[j], place.to("core", 0))

        def start(self, product):
            plus, minus = place.to("x", 1), place.to("x", -1)
            sums, landed = self.sums, self.landed
            for j, step in enumerate((2, 1, 3, 0)):
                parts = [product((x + step) % RING, core, side) for side in (0, 1)]
                self.net.arrived(10 + j, self.into.at[j])
                for side in (0, 1):
                    total = parts[side] + self.into[j, rows_of(side), :].astype(F32)
                    if j == 3:
                        self.last[rows_of(side), :] = total
                    else:
                        sums[j, rows_of(side), :] = total.astype(BF16)
                if j == 0:
                    self.net.send(14, sums.at[0, rows_of(0)], landed.at[0], plus)
                    self.net.send(15, sums.at[0, rows_of(1)], landed.at[1], minus)
                if j == 1:
                    self.net.send(16, sums.at[1, rows_of(1)], landed.at[2], plus)
                if j == 2:
                    self.net.send(17, sums.at[2, rows_of(0)], landed.at[3], minus)

        def forward(self):
            plus, minus = place.to("x", 1), place.to("x", -1)
            for side, device in ((0, plus), (1, minus)):
                self.net.arrived(14 + side, self.landed.at[side])
                total = self.sums[1 + side, rows_of(side), :].astype(F32) + self.landed[side].astype(F32)
                self.combined[side] = total.astype(BF16)
                self.net.send(18 + side, self.combined.at[side], self.landed.at[4 + side], device)

        def result(self, base, store):
            self.net.arrived(16, self.landed.at[2])
            self.net.arrived(17, self.landed.at[3])
            for side in (0, 1):
                self.net.arrived(18 + side, self.landed.at[4 + side])
                total = (
                    self.last[rows_of(side), :]
                    + self.landed[3 - side].astype(F32)
                    + self.landed[4 + side].astype(F32)
                )
                store(side, (base(side).astype(F32) + total).astype(BF16))

    r_mix, r_ffn = Summed(0), Summed(1)

    g_mix.p1_own()
    s_in.start()
    g_a.p1_own()
    g_mix.p1_forward()
    g_b.p1_own()
    take(blocks_a, mix_gain, mine, first=True)
    g_mix.p2_own()
    g_down.p1_own()
    s_in.from_core(6, 0)
    take(blocks_a, mix_gain, s_in.index(0, other=True))
    s_in.forward()
    g_mix.p2_forward()
    g_a.p1_forward()
    g_b.p1_forward()
    g_down.p1_forward()
    s_in.near()
    for step in (3, 1):
        take(blocks_a, mix_gain, s_in.index(step))
    s_in.far()
    take(blocks_a, mix_gain, s_in.index(2))
    for k, step in ((7, 3), (8, 1), (9, 2)):
        s_in.from_core(k, step)
        take(blocks_a, mix_gain, s_in.index(step, other=True))
    row_rates()
    g_a.p2_own()
    g_mix.finish()

    pooled = jnp.dot(
        scaled[...], mixer[:, :, 0:128, :].reshape(2048, 128), preferred_element_type=F32
    )
    pooled = (pooled * rates[...]).astype(BF16)
    reach = jnp.where(x == 0, 2, jnp.where(x == 1, 4, jnp.where(x == 2, 8, 16)))
    query = lax.broadcasted_iota(jnp.int32, (SEQ, SEQ), 0)
    earlier = lax.broadcasted_iota(jnp.int32, (SEQ, SEQ), 1)
    inside = jnp.where((earlier <= query) & (earlier > query - reach), 1.0, 0.0).astype(BF16)
    counts = jnp.minimum(query + 1, reach).astype(F32)
    scale = pool_s[...].astype(F32)
    for s in range(tokens // SEQ):
        rows = slice(s * SEQ, s * SEQ + SEQ)
        part = pooled[rows]
        window = jnp.dot(inside, part, preferred_element_type=F32)
        contrast = (window / counts - part.astype(F32)).astype(BF16)
        mixed = jnp.dot(contrast, pool_w[0], preferred_element_type=F32)
        group_out[rows, :] = (mixed * scale).astype(BF16)

    def mix_product(owner_x, owner_core, side):
        pair = mixer[owner_x, pl.ds(2 * owner_core, 2), 128:256, :]
        weights = jnp.concatenate([pair[0], pair[1]], axis=1)
        return jnp.dot(group_out[rows_of(side), :], weights, preferred_element_type=F32)

    r_mix.pair(mix_product)
    g_b.p2_own()
    r_mix.start(mix_product)
    r_mix.forward()
    g_a.p2_forward()

    def store_middle(side, value):
        blocks_b[mine, rows_of(side), :] = value

    r_mix.result(lambda side: stream[rows_of(side), :], store_middle)
    s_mid.start()
    g_b.p2_forward()
    g_down.p2_own()
    take(blocks_b, ffn_gain, mine, first=True)
    s_mid.from_core(6, 0)
    take(blocks_b, ffn_gain, s_mid.index(0, other=True))
    s_mid.forward()
    s_mid.near()
    for step in (3, 1):
        take(blocks_b, ffn_gain, s_mid.index(step))
    s_mid.far()
    take(blocks_b, ffn_gain, s_mid.index(2))
    for k, step in ((7, 3), (8, 1), (9, 2)):
        s_mid.from_core(k, step)
        take(blocks_b, ffn_gain, s_mid.index(step, other=True))
    row_rates()

    def units(buf, at, width, column):
        weights = buf[:, :, :, at : at + 2 * width].reshape(2048, 2 * width)

        def some(i, carry):
            rows = pl.ds(pl.multiple_of(i * 256, 256), 256)
            acts = jnp.dot(scaled[rows, :], weights, preferred_element_type=F32)
            rate = rates[rows, 0:width]
            gate, up = acts[:, :width] * rate, acts[:, width:] * rate
            hidden[rows, column : column + width] = (gate / (1.0 + jnp.exp(-gate)) * up).astype(BF16)
            return carry

        lax.fori_loop(0, tokens // 256, some, 0)

    g_a.finish()
    for chunk in range(3):
        units(pair_a, 256 * chunk, 128, 128 * chunk)
    g_down.p2_forward()
    g_b.finish()
    for chunk in range(2):
        units(pair_b, 256 * chunk, 128, 384 + 128 * chunk)
    units(pair_b, 512, 64, 640)
    g_down.finish()

    def ffn_product(owner_x, owner_core, side):
        pair = down[owner_x, pl.ds(2 * owner_core, 2)]
        weights = jnp.concatenate([pair[0], pair[1]], axis=1)
        return jnp.dot(hidden[rows_of(side), :], weights, preferred_element_type=F32)

    r_ffn.pair(ffn_product)
    r_ffn.start(ffn_product)
    r_ffn.forward()

    def store_result(side, value):
        out[rows_of(side), :] = value

    r_ffn.result(lambda side: blocks_b[mine, rows_of(side), :], store_result)

    for net in [g.net for g in gathers] + [s_in.net, s_mid.net, r_mix.net, r_ffn.net]:
        net.drain()


def on_device(stream, in_weight, pool_weight, pool_scale, out_weight, mix_gain, ffn_gain, gate_weight, up_weight, down_weight):
    tokens = stream.shape[0]
    half = tokens // 2
    return pl.pallas_call(
        kernel,
        out_shape=jax.ShapeDtypeStruct(stream.shape, BF16),
        in_specs=[pl.BlockSpec(memory_space=pltpu.VMEM)] * 10,
        out_specs=pl.BlockSpec(memory_space=pltpu.VMEM),
        scratch_shapes=[
            pltpu.VMEM((4, 4, 256, 128), BF16),
            pltpu.VMEM((4, 4, 128, 768), BF16),
            pltpu.VMEM((4, 4, 128, 640), BF16),
            pltpu.VMEM((4, 4, 704, 128), BF16),
            pltpu.VMEM((8, tokens, 256), BF16),
            pltpu.VMEM((8, tokens, 256), BF16),
            pltpu.VMEM((tokens, 2048), BF16),
            pltpu.VMEM((tokens, 128), F32),
            pltpu.VMEM((tokens, 128), F32),
            pltpu.VMEM((tokens, 128), BF16),
            pltpu.VMEM((tokens, 704), BF16),
            pltpu.VMEM((2, 4, tokens, 256), BF16),
            pltpu.VMEM((2, 4, tokens, 256), BF16),
            pltpu.VMEM((2, 3, tokens, 256), BF16),
            pltpu.VMEM((tokens, 256), F32),
            pltpu.VMEM((2, 2, half, 256), BF16),
            pltpu.VMEM((2, 6, half, 256), BF16),
            pltpu.SemaphoreType.DMA((4, 20)),
            pltpu.SemaphoreType.DMA((4, 20)),
            pltpu.SemaphoreType.DMA((2, 20)),
            pltpu.SemaphoreType.DMA((2, 20)),
        ],
        compiler_params=pltpu.CompilerParams(
            collective_id=0, has_side_effects=True, vmem_limit_bytes=60 * 1024 * 1024
        ),
    )(
        stream, in_weight, pool_weight, pool_scale.reshape(1, -1), out_weight,
        mix_gain.reshape(1, -1), ffn_gain.reshape(1, -1), gate_weight, up_weight, down_weight,
    )


def solution(mesh):
    finer = Mesh(
        mesh.devices.reshape(mesh.shape["rep"], RING, RING, RING, 2),
        ("rep", "fs_0", "fs_1", "x", "core"),
    )
    fs, tp = ("fs_0", "fs_1"), ("x", "core")
    rows = ("rep", *fs)
    return jax.shard_map(
        on_device,
        mesh=finer,
        in_specs=(
            P(rows, tp), P(fs, tp), P(tp, None, None), P(tp), P(tp, fs),
            P(), P(), P(fs, tp), P(fs, tp), P(tp, fs),
        ),
        out_specs=P(rows, tp),
        check_vma=False,
    )
```

time: 241 us -> 86.9 us (0.36); the launches traced: 237 us -> 86.8 us
  blocking collectives: 117 us -> 0 us
  Pallas kernels: 0 us -> 80.6 us
  waiting for transfers between devices: 59.7 us -> 0 us
  starting transfers between devices: 15.5 us -> 0 us
  matrix products: 15 us -> 0 us
  between operations: 13.7 us -> 0.01 us
  other arithmetic: 6.62 us -> 0 us
  local copies, waits for them, and re-layouts: 9.63 us -> 6.17 us
    all_to_all x3 -> x0, blocking collectives: 97.7 us -> none  [the longest x2 64.1 us: sum_at_owner(): lax.all_to_all(parts, axis, split_axis=0, concat_axis=0, tiled=True)]
    pallas_call x0 -> x1, Pallas kernels: none -> 80.6 us  [on_device(): pl.pallas_call(kernel, out_shape=jax.ShapeDtypeStruct(stream.shape, BF16)...]
    all_to_all x3 -> x0, waiting for transfers between devices: 59.6 us -> none  [sent_to_all(): lax.all_to_all(jnp.broadcast_to(array[None], (length, *array.shape)), axi...]
    all_gather x1 -> x0, blocking collectives: 19.2 us -> none  [all_blocks(): parts = lax.all_gather(parts, axes[k])]
    all_to_all x3 -> x0, starting transfers between devices: 15.5 us -> none  [sent_to_all(): lax.all_to_all(jnp.broadcast_to(array[None], (length, *array.shape)), axi...]
    dot_general x5 -> x0, matrix products: 15 us -> none  [the longest x1 7.65 us: on_device(): jnp.dot(hidden, gather_axes(down_weight, FS, (0, 1), 1), preferred_elemen...]
    unnamed x18 -> x7, local copies, waits for them, and re-layouts: 0.29 us -> 4.27 us
    transpose x1 -> x0, local copies, waits for them, and re-layouts: 3.67 us -> none  [all_blocks(): parts = parts.transpose(*back, *range(len(axes), parts.ndim))]
  transfers between devices with their start and end apart: 5 -> 0, of which waited for: 3 -> 0; matrix products, arithmetic and copies ran while one was open for 6% -> 0% of each run, Pallas kernels for 0% -> 0%
where the time goes in v1:
time: 86.9 us; the launch traced here: 86.8 us
  Pallas kernels  80.6 us (93%)
  local copies, waits for them, and re-layouts  6.17 us (7%)
    pallas_call x1, Pallas kernels, on_device(): pl.pallas_call(kernel, out_shape=jax.ShapeDtypeStruct(stream.shape, BF16)...  80.6 us
    unnamed x7, local copies, waits for them, and re-layouts  4.27 us

profile of v1, /device:TPU:1, one launch (start us, length us, event | category | flops | bytes accessed | tf_op | source)
XLA Modules:
  0.0 86.8 jit_solution(14737095069211167999)
XLA Ops:
  0.0 0.0 copy-start.1
  0.0 1.3 %reshape.10.mix_gain = bf16[1,2048]{1,0:T(2,128)(2,1)} reshape(bf16[2048]{0:T(1024)(128)(2,1)} %param.15) | data formatting | bytes 8192 | tf_op jit(solution)/shard_map/reshape | solution.py:430
  1.3 0.0 copy-done.1
  1.3 0.6 reshape.11.ffn_gain
  1.9 0.0 copy-start
  1.9 1.8 %copy.11.w_gate = bf16[128,704]{1,0:T(8,128)(2,1)} copy(bf16[128,704]{0,1:T(8,128)(2,1)} %param.17) | data formatting | bytes 360448 | tf_op args[7]
  3.7 0.0 copy-done
  3.7 0.8 copy.12.w_up
  4.5 80.6 %shard_map.100 = bf16[512,256]{1,0:T(8,128)(2,1)} custom-call(bf16[512,256]{1,0:T(8,128)(2,1)} %stream.1, bf16[128,128]{1,0:T(8,128)(2,1)} %w_in.1, bf16[1,128,128]{2,1,0:T(8,128)(2,1)} %pool_w.1, bf16[1,128]{1,0:T(2,128)(2,1)} %bitcast.1, bf16[128,128]{1,0:T(8,128)(2,1)} %w_out.1, bf16[1,2048]{1,0:T(2,128)(2,1)} %reshape.10.mix_gain, ...), custom_call_target="tpu_custom_call" | custom-call | tf_op jit(solution)/shard_map/pallas_call | solution.py:397
  85.1 1.7 %copy.14 = bf16[512,256]{1,0:T(8,128)(2,1)} copy(bf16[512,256]{1,0:T(8,128)(2,1)} %shard_map.100) | data formatting | bytes 524288
Async XLA Ops:
  0.0 1.3 %copy-start.1 = (bf16[2048]{0:T(1024)(128)(2,1)S(1)}, bf16[2048]{0:T(1024)(128)(2,1)}, u32[]{:S(2)}) copy-start(bf16[2048]{0:T(1024)(128)(2,1)} %param.16) | copy-start | bytes 12292
  1.9 1.8 %copy-start = (bf16[128,704]{0,1:T(8,128)(2,1)S(1)}, bf16[128,704]{0,1:T(8,128)(2,1)}, u32[]{:S(2)}) copy-start(bf16[128,704]{0,1:T(8,128)(2,1)} %param.18) | copy-start | bytes 540676

commit v2 on v1

--- a/solution.py
+++ b/solution.py
@@ -161,9 +161,9 @@
 
 
 def kernel(
-    stream, w_in, pool_w, pool_s, w_out, mix_gain, ffn_gain, w_gate, w_up, w_down, out,
-    mixer, pair_a, pair_b, down, blocks_a, blocks_b, scaled, squares, rates, group_out, hidden,
-    pair_out, pair_in, sums, last, combined, landed, gs, gr, xs, xr,
+    stream, w_in, pool_w_in, pool_s_in, w_out, mix_gain_in, ffn_gain_in, w_gate, w_up, w_down, out,
+    gains, mix_gain, ffn_gain, gate_in, up_in, pool_w, pool_s, mixer, pair_a, pair_b, down, blocks_a, blocks_b, scaled, squares, rates, group_out, hidden,
+    pair_out, pair_in, sums, last, combined, landed, fetched, gs, gr, xs, xr,
 ):
     place = Place()
     x, core, y, z = place.x, place.core, place.y, place.z
@@ -176,17 +176,23 @@
     for device in neighbours:
         pl.semaphore_signal(barrier, inc=1, device_id=device, device_id_type=pl.DeviceIdType.MESH)
 
-    mixer[z, y, 0:128, :] = w_in[...]
-    mixer[z, y, 128:256, :] = w_out[...]
-    blocks_a[mine] = stream[...]
-    for tile in range(5):
-        buf, at = (pair_a, tile) if tile < 3 else (pair_b, tile - 3)
-        lanes = slice(128 * tile, 128 * tile + 128)
-        buf[z, y, :, 256 * at : 256 * at + 128] = w_gate[:, lanes]
-        buf[z, y, :, 256 * at + 128 : 256 * at + 256] = w_up[:, lanes]
-    pair_b[z, y, :, 512:640] = jnp.concatenate([w_gate[:, 640:704], w_up[:, 640:704]], axis=1)
-    down[z, y] = w_down[...]
-
+    fetches = [
+        pltpu.make_async_copy(src, dst, fetched.at[i])
+        for i, (src, dst) in enumerate((
+            (stream, blocks_a.at[mine]),
+            (w_in, mixer.at[z, y, pl.ds(0, 128), :]),
+            (w_out, mixer.at[z, y, pl.ds(128, 128), :]),
+            (w_gate, gate_in),
+            (w_up, up_in),
+            (w_down, down.at[z, y]),
+            (mix_gain_in, gains.at[0]),
+            (ffn_gain_in, gains.at[1]),
+            (pool_w_in, pool_w),
+            (pool_s_in, pool_s),
+        ))
+    ]
+    for fetch in fetches:
+        fetch.start()
     pl.semaphore_wait(barrier, len(neighbours))
 
     gathers = [
@@ -198,7 +204,7 @@
 
     def take(buf, gain_ref, index, first=False):
         lanes = pl.ds(pl.multiple_of(index * 256, 256), 256)
-        gain = gain_ref[:, lanes].astype(F32)
+        gain = jnp.concatenate([gain_ref[pl.ds(2 * index + i, 1), :] for i in (0, 1)], axis=1)
 
         def some(i, carry):
             rows = pl.ds(pl.multiple_of(i * 64, 64), 64)
@@ -273,8 +279,23 @@
 
     r_mix, r_ffn = Summed(0), Summed(1)
 
+    fetches[0].wait()
+    s_in.start()
+    fetches[1].wait()
+    fetches[2].wait()
     g_mix.p1_own()
-    s_in.start()
+    fetches[3].wait()
+    fetches[4].wait()
+    for tile in range(5):
+        buf, at = (pair_a, tile) if tile < 3 else (pair_b, tile - 3)
+        some = slice(128 * tile, 128 * tile + 128)
+        buf[z, y, :, 256 * at : 256 * at + 128] = gate_in[some, :].T
+        buf[z, y, :, 256 * at + 128 : 256 * at + 256] = up_in[some, :].T
+    pair_b[z, y, :, 512:640] = jnp.concatenate([gate_in[640:704, :], up_in[640:704, :]], axis=0).T
+    for fetch in fetches[5:]:
+        fetch.wait()
+    mix_gain[...] = gains[0].astype(F32)
+    ffn_gain[...] = gains[1].astype(F32)
     g_a.p1_own()
     g_mix.p1_forward()
     g_b.p1_own()
@@ -332,7 +353,7 @@
     def store_middle(side, value):
         blocks_b[mine, rows_of(side), :] = value
 
-    r_mix.result(lambda side: stream[rows_of(side), :], store_middle)
+    r_mix.result(lambda side: blocks_a[mine, rows_of(side), :], store_middle)
     s_mid.start()
     g_b.p2_forward()
     g_down.p2_own()
@@ -397,9 +418,16 @@
     return pl.pallas_call(
         kernel,
         out_shape=jax.ShapeDtypeStruct(stream.shape, BF16),
-        in_specs=[pl.BlockSpec(memory_space=pltpu.VMEM)] * 10,
+        in_specs=[pl.BlockSpec(memory_space=pltpu.HBM)] * 10,
         out_specs=pl.BlockSpec(memory_space=pltpu.VMEM),
         scratch_shapes=[
+            pltpu.VMEM((2, 16, 128), BF16),
+            pltpu.VMEM((16, 128), F32),
+            pltpu.VMEM((16, 128), F32),
+            pltpu.VMEM((704, 128), BF16),
+            pltpu.VMEM((704, 128), BF16),
+            pltpu.VMEM((1, 128, 128), BF16),
+            pltpu.VMEM((1, 128), BF16),
             pltpu.VMEM((4, 4, 256, 128), BF16),
             pltpu.VMEM((4, 4, 128, 768), BF16),
             pltpu.VMEM((4, 4, 128, 640), BF16),
@@ -417,18 +445,19 @@
             pltpu.VMEM((tokens, 256), F32),
             pltpu.VMEM((2, 2, half, 256), BF16),
             pltpu.VMEM((2, 6, half, 256), BF16),
+            pltpu.SemaphoreType.DMA((10,)),
             pltpu.SemaphoreType.DMA((4, 20)),
             pltpu.SemaphoreType.DMA((4, 20)),
             pltpu.SemaphoreType.DMA((2, 20)),
             pltpu.SemaphoreType.DMA((2, 20)),
         ],
         compiler_params=pltpu.CompilerParams(
-            collective_id=0, has_side_effects=True, vmem_limit_bytes=60 * 1024 * 1024
+            collective_id=0, has_side_effects=True, vmem_limit_bytes=40 * 1024 * 1024
         ),
-    )(
+    )(*(pltpu.with_memory_space_constraint(a, pltpu.HBM) for a in (
         stream, in_weight, pool_weight, pool_scale.reshape(1, -1), out_weight,
-        mix_gain.reshape(1, -1), ffn_gain.reshape(1, -1), gate_weight, up_weight, down_weight,
-    )
+        mix_gain.reshape(16, 128), ffn_gain.reshape(16, 128), gate_weight.T, up_weight.T, down_weight,
+    )))
 
 
 def solution(mesh):

time: 86.9 us -> 79.5 us (0.915)
  local copies, waits for them, and re-layouts: 6.17 us -> 0.71 us
  Pallas kernels: 80.6 us -> 78.7 us
    unnamed x7 -> x1, local copies, waits for them, and re-layouts: 4.27 us -> 0.71 us
    pallas_call x1, Pallas kernels: 80.6 us -> 78.7 us  [on_device(): pl.pallas_call(kernel, out_shape=jax.ShapeDtypeStruct(stream.shape, BF16)...]
    reshape x2 -> x0, local copies, waits for them, and re-layouts: 1.9 us -> none  [the longest x1 1.3 us: on_device(): mix_gain.reshape(1, -1)]
where the time goes in v2:
time: 79.5 us; the launch traced here: 79.4 us
  Pallas kernels  78.7 us (99%)
    pallas_call x1, Pallas kernels, on_device(): pl.pallas_call(kernel, out_shape=jax.ShapeDtypeStruct(stream.shape, BF16)...  78.7 us

profile of v2, /device:TPU:1, one launch (start us, length us, event | category | flops | bytes accessed | tf_op | source)
XLA Modules:
  0.0 79.4 jit_solution(16861383768877042817)
XLA Ops:
  0.0 78.7 %shard_map.100 = bf16[512,256]{1,0:T(8,128)(2,1)S(1)} custom-call(bf16[512,256]{1,0:T(8,128)(2,1)} %stream.1, bf16[128,128]{1,0:T(8,128)(2,1)} %w_in.1, bf16[1,128,128]{2,1,0:T(8,128)(2,1)} %pool_w_in.1, bf16[1,128]{1,0:T(2,128)(2,1)} %bitcast.9, bf16[128,128]{1,0:T(8,128)(2,1)} %w_out.1, bf16[16,128]{1,0:T(8,128)(2,1)} %bitcast.7, bf16[16,128]{1,0:T(8,128)(2,1)} %bitcast.8, ...), custom_call_target="tpu_custom_call" | custom-call | tf_op jit(solution)/shard_map/pallas_call | solution.py:418
  78.7 0.7 copy.12

commit v3 on v2

v3 whole, which is shorter than its diff:
```python
import jax
import jax.numpy as jnp
from jax import lax
from jax.experimental import pallas as pl
from jax.experimental.pallas import tpu as pltpu
from jax.sharding import Mesh
from jax.sharding import PartitionSpec as P

SEQ = 128
RING = 4
EPS = 1e-06
F32, BF16 = jnp.float32, jnp.bfloat16


class Place:
    def __init__(self):
        self.rep, self.z, self.y = (lax.axis_index(a) for a in ("rep", "fs_0", "fs_1"))
        self.x, self.core = lax.axis_index("x"), lax.axis_index("core")

    def to(self, axis, step):
        if axis == "core":
            return {"core": 1 - self.core}
        if axis == "z":
            deep = (self.rep * RING + self.z + step + 2 * RING) % (2 * RING)
            return {"rep": deep // RING, "fs_0": deep % RING}
        index = {"x": self.x, "y": self.y}[axis]
        return {{"x": "x", "y": "fs_1"}[axis]: (index + step + RING) % RING}


class Net:
    def __init__(self, place, fresh):
        self.place, self.fresh = place, fresh

    def send(self, src, dst, sent, landed, axis, step):
        pltpu.make_async_remote_copy(
            src_ref=src,
            dst_ref=dst,
            send_sem=sent,
            recv_sem=landed,
            device_id=self.place.to(axis, step),
            device_id_type=pl.DeviceIdType.MESH,
        ).start()

    def wait(self, semaphore, as_many):
        pltpu.make_async_copy(as_many, as_many, semaphore).wait()


class Gather(Net):
    def __init__(self, place, fresh, buf):
        super().__init__(place, fresh)
        self.buf = buf
        half = buf.shape[2] // 2
        self.flows = (("y", "z", 0, half), ("z", "y", half, half))
        self.sent_1, self.sent_2, self.got_own, self.got_line, self.got_plane, self.got_all = (
            fresh() for _ in range(6)
        )

    def block(self, axis, step, first, rows):
        z, y = self.place.z, self.place.y
        z, y = ((z + step) % RING, y) if axis == "z" else (z, (y + step) % RING)
        return self.buf.at[z, y, pl.ds(first, rows), :]

    def plane(self, axis, step, side, first, rows):
        two = pl.ds(2 * side, 2)
        if axis == "z":
            return self.buf.at[(self.place.z + step) % RING, two, pl.ds(first, rows), :]
        return self.buf.at[two, (self.place.y + step) % RING, pl.ds(first, rows), :]

    def relay(self, part, sent, landed, axis, step):
        self.send(part, part, sent, landed, axis, step)

    def p1_own(self):
        for axis, _, first, rows in self.flows:
            own = self.block(axis, 0, first, rows)
            self.relay(own, self.sent_1, self.got_own, axis, 1)
            self.relay(own, self.sent_1, self.got_own, axis, -1)

    def p1_forward(self):
        self.wait(self.got_own, self.buf.at[0, pl.ds(0, 2)])
        for axis, _, first, rows in self.flows:
            half = (rows // 2 + 15) // 16 * 16
            self.relay(self.block(axis, 3, first, half), self.sent_1, self.got_line, axis, 1)
            self.relay(self.block(axis, 1, first + half, rows - half), self.sent_1, self.got_line, axis, -1)

    def p2_own(self):
        self.p2_first()
        self.p2_second()

    def p2_first(self):
        self.wait(self.got_line, self.buf.at[0, 0])
        for _, axis, first, rows in self.flows:
            low, high = (self.plane(axis, 0, side, first, rows) for side in (0, 1))
            self.relay(low, self.sent_2, self.got_plane, axis, 1)
            self.relay(high, self.sent_2, self.got_plane, axis, -1)

    def p2_second(self):
        for _, axis, first, rows in self.flows:
            low, high = (self.plane(axis, 0, side, first, rows) for side in (0, 1))
            self.relay(high, self.sent_2, self.got_all, axis, 1)
            self.relay(low, self.sent_2, self.got_all, axis, -1)

    def p2_forward(self):
        self.wait(self.got_plane, self.buf.at[0])
        for _, axis, first, rows in self.flows:
            self.relay(self.plane(axis, 3, 0, first, rows), self.sent_2, self.got_all, axis, 1)
            self.relay(self.plane(axis, 1, 1, first, rows), self.sent_2, self.got_all, axis, -1)

    def finish(self):
        self.wait(self.got_all, self.buf.at[pl.ds(0, 2)])

    def drain(self):
        self.wait(self.sent_1, self.buf.at[0, pl.ds(0, 3)])
        self.wait(self.sent_2, self.buf.at[pl.ds(0, 3)])


class Spread(Net):
    def __init__(self, place, fresh, buf, first, rows):
        super().__init__(place, fresh)
        self.buf, self.first, self.rows = buf, first, rows
        self.sent, self.got_0, self.got_1, self.got_2, self.pair_0, self.pair_1, self.pair_2 = (
            fresh() for _ in range(7)
        )

    def index(self, step, other=False):
        core = 1 - self.place.core if other else self.place.core
        return 2 * ((self.place.x + step) % RING) + core

    def relay(self, step, side, landed, to):
        half = self.rows // 2
        part = self.buf.at[self.index(step), pl.ds(self.first + side * half, half), :]
        self.send(part, part, self.sent, landed, "x", to)

    def to_core(self, step, landed):
        block = self.buf.at[self.index(step), pl.ds(self.first, self.rows), :]
        self.send(block, block, self.sent, landed, "core", 0)

    def blocks(self, count):
        return self.buf.at[pl.ds(0, count), pl.ds(self.first, self.rows), :]

    def start(self):
        self.relay(0, 0, self.got_0, 1)
        self.relay(0, 1, self.got_0, -1)
        self.relay(0, 1, self.got_1, 1)
        self.relay(0, 0, self.got_1, -1)
        self.to_core(0, self.pair_0)

    def forward(self):
        self.wait(self.got_0, self.blocks(1))
        self.relay(3, 0, self.got_2, 1)
        self.relay(1, 1, self.got_2, -1)

    def near(self):
        self.wait(self.got_1, self.blocks(1))
        self.to_core(3, self.pair_1)
        self.to_core(1, self.pair_1)

    def far(self):
        self.wait(self.got_2, self.blocks(1))
        self.to_core(2, self.pair_2)

    def other_own(self):
        self.wait(self.pair_0, self.blocks(1))

    def other_near(self):
        self.wait(self.pair_1, self.blocks(2))

    def other_far(self):
        self.wait(self.pair_2, self.blocks(1))

    def drain(self):
        self.wait(self.sent, self.blocks(7))


def kernel(
    stream, w_in, pool_w_in, pool_s_in, w_out, mix_gain_in, ffn_gain_in, w_gate, w_up, w_down, out,
    gains, mix_gain, ffn_gain, gate_in, up_in, down_in, pool_w, pool_s,
    mixer, pair_a, pair_b, down_a, down_b, blocks_a, blocks_b, scaled, squares, rates, group_out, hidden,
    out_0, in_0, sums_0, own_0, combined_0, landed_0,
    out_1, in_1, sums_1, own_1, combined_1, landed_1, total_1,
    out_2, in_2, sums_2, own_2, combined_2, landed_2,
    fetched, sems,
):
    place = Place()
    x, core, y, z = place.x, place.core, place.y, place.z
    mine = 2 * x + core
    tokens = stream.shape[0]

    barrier = pltpu.get_barrier_semaphore()
    neighbours = [place.to(a, s) for a in "xyz" for s in (1, -1)] + [place.to("core", 0)]
    for device in neighbours:
        pl.semaphore_signal(barrier, inc=1, device_id=device, device_id_type=pl.DeviceIdType.MESH)
    fetches = [
        pltpu.make_async_copy(src, dst, fetched.at[i])
        for i, (src, dst) in enumerate((
            (stream, blocks_a.at[mine]),
            (w_in, mixer.at[z, y, pl.ds(0, 128), :]),
            (w_out, mixer.at[z, y, pl.ds(128, 128), :]),
            (w_gate, gate_in),
            (w_up, up_in),
            (w_down, down_in),
            (mix_gain_in, gains.at[0]),
            (ffn_gain_in, gains.at[1]),
            (pool_w_in, pool_w),
            (pool_s_in, pool_s),
        ))
    ]
    for fetch in fetches:
        fetch.start()
    pl.semaphore_wait(barrier, len(neighbours))

    taken = iter(range(sems.shape[0]))

    def fresh():
        return sems.at[next(taken)]

    gathers = [Gather(place, fresh, buf) for buf in (mixer, pair_a, pair_b, down_a, down_b)]
    g_mix, g_a, g_b, g_da, g_db = gathers
    streams = (0, 1)
    rows_each = tokens // 2
    half = rows_each // 2
    s_in = [Spread(place, fresh, blocks_a, rows_each * t, rows_each) for t in streams]
    s_mid = [Spread(place, fresh, blocks_b, rows_each * t, rows_each) for t in streams]

    def take(spread, gain_ref, step, other=False, first=False):
        index = spread.index(step, other)
        lanes = pl.ds(pl.multiple_of(index * 256, 256), 256)
        gain = jnp.concatenate([gain_ref[pl.ds(2 * index + i, 1), :] for i in (0, 1)], axis=1)

        def some(i, carry):
            rows = pl.ds(pl.multiple_of(spread.first + i * 64, 64), 64)
            value = spread.buf[index, rows, :].astype(F32)
            scaled[rows, lanes] = (value * gain).astype(BF16)
            square = value * value
            square = square[:, :128] + square[:, 128:]
            squares[rows, :] = square if first else squares[rows, :] + square
            return carry

        lax.fori_loop(0, spread.rows // 64, some, 0)

    def row_rates(t):
        rows = slice(rows_each * t, rows_each * t + rows_each)
        total = jnp.sum(squares[rows, :], axis=1, keepdims=True)
        rates[rows, :] = jnp.broadcast_to(lax.rsqrt(total * (1.0 / 2048.0) + EPS), (rows_each, 128))

    def rows_of(side):
        return pl.ds(side * half, half)

    class Summed(Net):
        steps = (2, 1, 3, 0)

        def __init__(self, t, *buffers):
            super().__init__(place, fresh)
            self.out, self.into, self.sums, self.own, self.combined, self.landed = (
                buffer.at[t] for buffer in buffers
            )
            self.sent_pair, self.sent, self.pair_0, self.pair_1, self.got_far, self.got = (
                fresh() for _ in range(6)
            )

        def give(self):
            for j in range(4):
                landed = self.pair_1 if j else self.pair_0
                self.send(self.out.at[j], self.into.at[j], self.sent_pair, landed, "core", 0)

        def start(self):
            sums, landed = self.sums, self.landed
            for j in range(4):
                if j < 2:
                    self.wait(*((self.pair_0, self.into.at[0]), (self.pair_1, self.into.at[pl.ds(1, 3)]))[j])
                total = self.own[j] + self.into[j].astype(F32)
                if j == 3:
                    self.own[j] = total
                else:
                    sums[j] = total.astype(BF16)
                if j == 0:
                    self.send(sums.at[0, rows_of(0)], landed.at[0], self.sent, self.got_far, "x", 1)
                    self.send(sums.at[0, rows_of(1)], landed.at[1], self.sent, self.got_far, "x", -1)
                if j == 1:
                    self.send(sums.at[1, rows_of(1)], landed.at[2], self.sent, self.got, "x", 1)
                if j == 2:
                    self.send(sums.at[2, rows_of(0)], landed.at[3], self.sent, self.got, "x", -1)

        def forward(self):
            self.wait(self.got_far, self.landed.at[pl.ds(0, 2)])
            for side, step in ((0, 1), (1, -1)):
                total = self.sums[1 + side, rows_of(side), :].astype(F32) + self.landed[side].astype(F32)
                self.combined[side] = total.astype(BF16)
                self.send(self.combined.at[side], self.landed.at[4 + side], self.sent, self.got, "x", step)

        def result(self, store):
            self.wait(self.got, self.landed.at[pl.ds(2, 4)])
            for side in (0, 1):
                store(
                    side,
                    self.own[3, rows_of(side), :]
                    + self.landed[3 - side].astype(F32)
                    + self.landed[4 + side].astype(F32),
                )

        def drain(self):
            self.wait(self.sent_pair, self.out)
            self.wait(self.sent, self.sums)

    def pair_up(sums, products):
        for group in products.groups:
            for i, j, value in products(group, 1 - core):
                sums[i].out[j] = value.astype(BF16)
        for each in sums:
            each.give()
        for group in products.groups:
            for i, j, value in products(group, core):
                sums[i].own[j] = value

    r_mix = [Summed(t, out_0, in_0, sums_0, own_0, combined_0, landed_0) for t in streams]
    r_one = [Summed(t, out_1, in_1, sums_1, own_1, combined_1, landed_1) for t in streams]
    r_two = [Summed(t, out_2, in_2, sums_2, own_2, combined_2, landed_2) for t in streams]

    def token_rows(t, side):
        return pl.ds(rows_each * t + half * side, half)

    reach = jnp.where(x == 0, 2, jnp.where(x == 1, 4, jnp.where(x == 2, 8, 16)))

    def mix(t):
        first = rows_each * t
        pooled = jnp.dot(
            scaled[first : first + rows_each, :], mixer[:, :, 0:128, :].reshape(2048, 128),
            preferred_element_type=F32,
        )
        pooled = (pooled * rates[first : first + rows_each, :]).astype(BF16)
        query = lax.broadcasted_iota(jnp.int32, (SEQ, SEQ), 0)
        earlier = lax.broadcasted_iota(jnp.int32, (SEQ, SEQ), 1)
        inside = jnp.where((earlier <= query) & (earlier > query - reach), 1.0, 0.0).astype(BF16)
        counts = jnp.minimum(query + 1, reach).astype(F32)
        scale = pool_s[...].astype(F32)
        for s in range(rows_each // SEQ):
            part = pooled[s * SEQ : s * SEQ + SEQ]
            window = jnp.dot(inside, part, preferred_element_type=F32)
            contrast = (window / counts - part.astype(F32)).astype(BF16)
            mixed = jnp.dot(contrast, pool_w[0], preferred_element_type=F32)
            group_out[first + s * SEQ : first + s * SEQ + SEQ, :] = (mixed * scale).astype(BF16)

    def mix_products(t):
        first = rows_each * t

        def products(group, owner_core):
            for j in group:
                pair = mixer[(x + Summed.steps[j]) % RING, pl.ds(2 * owner_core, 2), 128:256, :]
                weights = jnp.concatenate([pair[0], pair[1]], axis=1)
                tokens_of = group_out[first : first + rows_each, :]
                yield 0, j, jnp.dot(tokens_of, weights, preferred_element_type=F32)

        products.groups = ((0,), (1,), (2,), (3,))
        return products

    def ffn_products(buf):
        def products(group, owner_core):
            columns = []
            for j in group:
                pair = buf[(x + Summed.steps[j]) % RING, pl.ds(2 * owner_core, 2)]
                early = jnp.concatenate([pair[0][:, :64], pair[1][:, :64]], axis=1)
                late = jnp.concatenate([pair[0][:, 64:], pair[1][:, 64:]], axis=1)
                columns.append(jnp.concatenate([early, late], axis=0))
            weights = jnp.concatenate(columns, axis=1)
            both = jnp.dot(hidden[...], weights, preferred_element_type=F32)
            for t in streams:
                for i, j in enumerate(group):
                    yield t, j, both[rows_each * t : rows_each * t + rows_each, 128 * i : 128 * i + 128]

        products.groups = ((0, 1), (2, 3))
        return products

    def units(t, buf, at, width, column):
        weights = buf[:, :, :, at : at + 2 * width].reshape(2048, 2 * width)
        rows = slice(rows_each * t, rows_each * t + rows_each)
        acts = jnp.dot(scaled[rows, :], weights, preferred_element_type=F32)
        rate = rates[rows, 0:width]
        gate, up = acts[:, :width] * rate, acts[:, width:] * rate
        hidden[rows, column : column + width] = (gate / (1.0 + jnp.exp(-gate)) * up).astype(BF16)

    def units_a(t):
        for chunk in range(3):
            units(t, pair_a, 256 * chunk, 128, 128 * chunk)

    def units_b(t):
        for chunk in range(2):
            units(t, pair_b, 256 * chunk, 128, 384 + 128 * chunk)
        units(t, pair_b, 512, 64, 640)

    def middle_of(t):
        def store(side, total):
            rows = token_rows(t, side)
            blocks_b[mine, rows, :] = (blocks_a[mine, rows, :].astype(F32) + total).astype(BF16)

        return store

    def first_of(t):
        def store(side, total):
            total_1[token_rows(t, side), :] = total

        return store

    def result_of(t):
        def store(side, second):
            rows = token_rows(t, side)
            first = total_1[rows, :]
            for i in (0, 1):
                lanes = slice(128 * i, 128 * i + 128)
                some = slice(64 * i, 64 * i + 64)
                total = jnp.concatenate([first[:, some], second[:, some]], axis=1)
                out[rows, lanes] = (blocks_b[mine, rows, lanes].astype(F32) + total).astype(BF16)

        return store

    fetches[0].wait()
    s_in[0].start()
    fetches[1].wait()
    fetches[2].wait()
    g_mix.p1_own()
    s_in[1].start()
    fetches[3].wait()
    fetches[4].wait()
    for tile in range(5):
        buf, at = (pair_a, tile) if tile < 3 else (pair_b, tile - 3)
        some = slice(128 * tile, 128 * tile + 128)
        buf[z, y, :, 256 * at : 256 * at + 128] = gate_in[some, :].T
        buf[z, y, :, 256 * at + 128 : 256 * at + 256] = up_in[some, :].T
    pair_b[z, y, :, 512:640] = jnp.concatenate([gate_in[640:704, :], up_in[640:704, :]], axis=0).T
    for fetch in fetches[5:]:
        fetch.wait()
    for lane, buf in ((0, down_a), (64, down_b)):
        some = slice(lane, lane + 64)
        buf[z, y] = jnp.concatenate([down_in[0:352, some], down_in[352:704, some]], axis=1)
    mix_gain[...] = gains[0].astype(F32)
    ffn_gain[...] = gains[1].astype(F32)
    g_a.p1_own()
    g_b.p1_own()
    for t in streams:
        take(s_in[t], mix_gain, 0, first=True)
    g_mix.p1_forward()
    g_da.p1_own()
    g_db.p1_own()
    s_in[0].forward()
    g_a.p1_forward()
    for t in streams:
        s_in[t].other_own()
        take(s_in[t], mix_gain, 0, other=True)
    g_mix.p2_own()
    g_b.p1_forward()
    s_in[0].near()
    s_in[1].forward()
    for step in (3, 1):
        take(s_in[0], mix_gain, step)
    s_in[1].near()
    g_mix.p2_forward()
    g_da.p1_forward()
    g_db.p1_forward()
    s_in[0].far()
    take(s_in[0], mix_gain, 2)
    for step in (3, 1):
        take(s_in[1], mix_gain, step)
    s_in[1].far()
    take(s_in[1], mix_gain, 2)
    g_a.p2_own()
    for t in streams:
        s_in[t].other_near()
        take(s_in[t], mix_gain, 3, other=True)
        take(s_in[t], mix_gain, 1, other=True)
        s_in[t].other_far()
        take(s_in[t], mix_gain, 2, other=True)
        row_rates(t)
    g_b.p2_own()
    g_mix.finish()
    mix(0)
    pair_up([r_mix[0]], mix_products(0))
    mix(1)
    r_mix[0].start()
    pair_up([r_mix[1]], mix_products(1))
    r_mix[1].start()
    r_mix[0].forward()
    r_mix[1].forward()
    r_mix[0].result(middle_of(0))
    s_mid[0].start()
    take(s_mid[0], ffn_gain, 0, first=True)
    g_a.p2_forward()
    g_b.p2_forward()
    r_mix[1].result(middle_of(1))
    s_mid[1].start()
    take(s_mid[1], ffn_gain, 0, first=True)
    g_da.p2_own()
    g_db.p2_first()
    for t in streams:
        s_mid[t].other_own()
        take(s_mid[t], ffn_gain, 0, other=True)
    s_mid[0].forward()
    s_mid[0].near()
    s_mid[1].forward()
    for step in (3, 1):
        take(s_mid[0], ffn_gain, step)
    s_mid[1].near()
    s_mid[0].far()
    take(s_mid[0], ffn_gain, 2)
    for step in (3, 1):
        take(s_mid[1], ffn_gain, step)
    s_mid[1].far()
    take(s_mid[1], ffn_gain, 2)
    for t in streams:
        s_mid[t].other_near()
        take(s_mid[t], ffn_gain, 3, other=True)
        take(s_mid[t], ffn_gain, 1, other=True)
        s_mid[t].other_far()
        take(s_mid[t], ffn_gain, 2, other=True)
        row_rates(t)
    g_a.finish()
    units_a(0)
    g_da.p2_forward()
    g_db.p2_second()
    units_a(1)
    g_b.finish()
    units_b(0)
    units_b(1)
    g_db.p2_forward()
    g_da.finish()
    pair_up(r_one, ffn_products(down_a))
    for t in streams:
        r_one[t].start()
    g_db.finish()
    pair_up(r_two, ffn_products(down_b))
    for t in streams:
        r_one[t].forward()
    for t in streams:
        r_two[t].start()
    for t in streams:
        r_one[t].result(first_of(t))
    for t in streams:
        r_two[t].forward()
    for t in streams:
        r_two[t].result(result_of(t))

    for net in [*gathers, *s_in, *s_mid, *r_mix, *r_one, *r_two]:
        net.drain()


def summing(tokens, width):
    rows = tokens // 2
    return [
        pltpu.VMEM((2, 4, rows, width), BF16),
        pltpu.VMEM((2, 4, rows, width), BF16),
        pltpu.VMEM((2, 3, rows, width), BF16),
        pltpu.VMEM((2, 4, rows, width), F32),
        pltpu.VMEM((2, 2, rows // 2, width), BF16),
        pltpu.VMEM((2, 6, rows // 2, width), BF16),
    ]


def on_device(stream, in_weight, pool_weight, pool_scale, out_weight, mix_gain, ffn_gain, gate_weight, up_weight, down_weight):
    tokens = stream.shape[0]
    return pl.pallas_call(
        kernel,
        out_shape=jax.ShapeDtypeStruct(stream.shape, BF16),
        in_specs=[pl.BlockSpec(memory_space=pltpu.HBM)] * 10,
        out_specs=pl.BlockSpec(memory_space=pltpu.VMEM),
        scratch_shapes=[
            pltpu.VMEM((2, 16, 128), BF16),
            pltpu.VMEM((16, 128), F32),
            pltpu.VMEM((16, 128), F32),
            pltpu.VMEM((704, 128), BF16),
            pltpu.VMEM((704, 128), BF16),
            pltpu.VMEM((704, 128), BF16),
            pltpu.VMEM((1, 128, 128), BF16),
            pltpu.VMEM((1, 128), BF16),
            pltpu.VMEM((4, 4, 256, 128), BF16),
            pltpu.VMEM((4, 4, 128, 768), BF16),
            pltpu.VMEM((4, 4, 128, 640), BF16),
            pltpu.VMEM((4, 4, 352, 128), BF16),
            pltpu.VMEM((4, 4, 352, 128), BF16),
            pltpu.VMEM((8, tokens, 256), BF16),
            pltpu.VMEM((8, tokens, 256), BF16),
            pltpu.VMEM((tokens, 2048), BF16),
            pltpu.VMEM((tokens, 128), F32),
            pltpu.VMEM((tokens, 128), F32),
            pltpu.VMEM((tokens, 128), BF16),
            pltpu.VMEM((tokens, 704), BF16),
            *summing(tokens, 256),
            *summing(tokens, 128),
            pltpu.VMEM((tokens, 128), F32),
            *summing(tokens, 128),
            pltpu.SemaphoreType.DMA((10,)),
            pltpu.SemaphoreType.DMA((94,)),
        ],
        compiler_params=pltpu.CompilerParams(
            collective_id=0, has_side_effects=True, vmem_limit_bytes=40 * 1024 * 1024
        ),
    )(*(pltpu.with_memory_space_constraint(a, pltpu.HBM) for a in (
        stream, in_weight, pool_weight, pool_scale.reshape(1, -1), out_weight,
        mix_gain.reshape(16, 128), ffn_gain.reshape(16, 128), gate_weight.T, up_weight.T, down_weight,
    )))


def solution(mesh):
    finer = Mesh(
        mesh.devices.reshape(mesh.shape["rep"], RING, RING, RING, 2),
        ("rep", "fs_0", "fs_1", "x", "core"),
    )
    fs, tp = ("fs_0", "fs_1"), ("x", "core")
    rows = ("rep", *fs)
    return jax.shard_map(
        on_device,
        mesh=finer,
        in_specs=(
            P(rows, tp), P(fs, tp), P(tp, None, None), P(tp), P(tp, fs),
            P(), P(), P(fs, tp), P(fs, tp), P(tp, fs),
        ),
        out_specs=P(rows, tp),
        check_vma=False,
    )
```

time: 79.5 us -> 72.5 us (0.912)
  Pallas kernels: 78.7 us -> 71.3 us
    pallas_call x1, Pallas kernels: 78.7 us -> 71.3 us  [on_device(): pl.pallas_call(kernel, out_shape=jax.ShapeDtypeStruct(stream.shape, BF16)...]
where the time goes in v3:
time: 72.5 us; the launch traced here: 72 us
  Pallas kernels  71.3 us (98%)
    pallas_call x1, Pallas kernels, on_device(): pl.pallas_call(kernel, out_shape=jax.ShapeDtypeStruct(stream.shape, BF16)...  71.3 us

profile of v3, /device:TPU:1, one launch (start us, length us, event | category | flops | bytes accessed | tf_op | source)
XLA Modules:
  0.0 72.0 jit_solution(13134213099079113638)
XLA Ops:
  0.0 71.3 %shard_map.100 = bf16[512,256]{1,0:T(8,128)(2,1)S(1)} custom-call(bf16[512,256]{1,0:T(8,128)(2,1)} %stream.1, bf16[128,128]{1,0:T(8,128)(2,1)} %w_in.1, bf16[1,128,128]{2,1,0:T(8,128)(2,1)} %pool_w_in.1, bf16[1,128]{1,0:T(2,128)(2,1)} %bitcast.9, bf16[128,128]{1,0:T(8,128)(2,1)} %w_out.1, bf16[16,128]{1,0:T(8,128)(2,1)} %bitcast.7, bf16[16,128]{1,0:T(8,128)(2,1)} %bitcast.8, ...), custom_call_target="tpu_custom_call" | custom-call | tf_op jit(solution)/shard_map/pallas_call | solution.py:557
  71.3 0.7 copy.12

commit v4 on v3

--- a/solution.py
+++ b/solution.py
@@ -28,14 +28,14 @@
 
 
 class Net:
-    def __init__(self, place, fresh):
-        self.place, self.fresh = place, fresh
-
-    def send(self, src, dst, sent, landed, axis, step):
+    def __init__(self, place, fresh, sent):
+        self.place, self.fresh, self.sent = place, fresh, sent
+
+    def send(self, src, dst, landed, axis, step):
         pltpu.make_async_remote_copy(
             src_ref=src,
             dst_ref=dst,
-            send_sem=sent,
+            send_sem=self.sent,
             recv_sem=landed,
             device_id=self.place.to(axis, step),
             device_id_type=pl.DeviceIdType.MESH,
@@ -46,13 +46,13 @@
 
 
 class Gather(Net):
-    def __init__(self, place, fresh, buf):
-        super().__init__(place, fresh)
+    def __init__(self, place, fresh, sent, buf):
+        super().__init__(place, fresh, sent)
         self.buf = buf
         half = buf.shape[2] // 2
         self.flows = (("y", "z", 0, half), ("z", "y", half, half))
-        self.sent_1, self.sent_2, self.got_own, self.got_line, self.got_plane, self.got_all = (
-            fresh() for _ in range(6)
+        self.got_own, self.got_line, self.got_plane, self.got_all = (
+            fresh() for _ in range(4)
         )
 
     def block(self, axis, step, first, rows):
@@ -66,21 +66,21 @@
             return self.buf.at[(self.place.z + step) % RING, two, pl.ds(first, rows), :]
         return self.buf.at[two, (self.place.y + step) % RING, pl.ds(first, rows), :]
 
-    def relay(self, part, sent, landed, axis, step):
-        self.send(part, part, sent, landed, axis, step)
+    def relay(self, part, landed, axis, step):
+        self.send(part, part, landed, axis, step)
 
     def p1_own(self):
         for axis, _, first, rows in self.flows:
             own = self.block(axis, 0, first, rows)
-            self.relay(own, self.sent_1, self.got_own, axis, 1)
-            self.relay(own, self.sent_1, self.got_own, axis, -1)
+            self.relay(own, self.got_own, axis, 1)
+            self.relay(own, self.got_own, axis, -1)
 
     def p1_forward(self):
         self.wait(self.got_own, self.buf.at[0, pl.ds(0, 2)])
         for axis, _, first, rows in self.flows:
             half = (rows // 2 + 15) // 16 * 16
-            self.relay(self.block(axis, 3, first, half), self.sent_1, self.got_line, axis, 1)
-            self.relay(self.block(axis, 1, first + half, rows - half), self.sent_1, self.got_line, axis, -1)
+            self.relay(self.block(axis, 3, first, half), self.got_line, axis, 1)
+            self.relay(self.block(axis, 1, first + half, rows - half), self.got_line, axis, -1)
 
     def p2_own(self):
         self.p2_first()
@@ -90,35 +90,31 @@
         self.wait(self.got_line, self.buf.at[0, 0])
         for _, axis, first, rows in self.flows:
             low, high = (self.plane(axis, 0, side, first, rows) for side in (0, 1))
-            self.relay(low, self.sent_2, self.got_plane, axis, 1)
-            self.relay(high, self.sent_2, self.got_plane, axis, -1)
+            self.relay(low, self.got_plane, axis, 1)
+            self.relay(high, self.got_plane, axis, -1)
 
     def p2_second(self):
         for _, axis, first, rows in self.flows:
             low, high = (self.plane(axis, 0, side, first, rows) for side in (0, 1))
-            self.relay(high, self.sent_2, self.got_all, axis, 1)
-            self.relay(low, self.sent_2, self.got_all, axis, -1)
+            self.relay(high, self.got_all, axis, 1)
+            self.relay(low, self.got_all, axis, -1)
 
     def p2_forward(self):
         self.wait(self.got_plane, self.buf.at[0])
         for _, axis, first, rows in self.flows:
-            self.relay(self.plane(axis, 3, 0, first, rows), self.sent_2, self.got_all, axis, 1)
-            self.relay(self.plane(axis, 1, 1, first, rows), self.sent_2, self.got_all, axis, -1)
+            self.relay(self.plane(axis, 3, 0, first, rows), self.got_all, axis, 1)
+            self.relay(self.plane(axis, 1, 1, first, rows), self.got_all, axis, -1)
 
     def finish(self):
         self.wait(self.got_all, self.buf.at[pl.ds(0, 2)])
 
-    def drain(self):
-        self.wait(self.sent_1, self.buf.at[0, pl.ds(0, 3)])
-        self.wait(self.sent_2, self.buf.at[pl.ds(0, 3)])
-
 
 class Spread(Net):
-    def __init__(self, place, fresh, buf, first, rows):
-        super().__init__(place, fresh)
+    def __init__(self, place, fresh, sent, buf, first, rows):
+        super().__init__(place, fresh, sent)
         self.buf, self.first, self.rows = buf, first, rows
-        self.sent, self.got_0, self.got_1, self.got_2, self.pair_0, self.pair_1, self.pair_2 = (
-            fresh() for _ in range(7)
+        self.got_0, self.got_1, self.got_2, self.pair_0, self.pair_1, self.pair_2 = (
+            fresh() for _ in range(6)
         )
 
     def index(self, step, other=False):
@@ -128,11 +124,11 @@
     def relay(self, step, side, landed, to):
         half = self.rows // 2
         part = self.buf.at[self.index(step), pl.ds(self.first + side * half, half), :]
-        self.send(part, part, self.sent, landed, "x", to)
+        self.send(part, part, landed, "x", to)
 
     def to_core(self, step, landed):
         block = self.buf.at[self.index(step), pl.ds(self.first, self.rows), :]
-        self.send(block, block, self.sent, landed, "core", 0)
+        self.send(block, block, landed, "core", 0)
 
     def blocks(self, count):
         return self.buf.at[pl.ds(0, count), pl.ds(self.first, self.rows), :]
@@ -167,18 +163,15 @@
     def other_far(self):
         self.wait(self.pair_2, self.blocks(1))
 
-    def drain(self):
-        self.wait(self.sent, self.blocks(7))
-
 
 def kernel(
     stream, w_in, pool_w_in, pool_s_in, w_out, mix_gain_in, ffn_gain_in, w_gate, w_up, w_down, out,
     gains, mix_gain, ffn_gain, gate_in, up_in, down_in, pool_w, pool_s,
-    mixer, pair_a, pair_b, down_a, down_b, blocks_a, blocks_b, scaled, squares, rates, group_out, hidden,
+    mixer_in, mixer_out, pair_a, pair_b, down_a, down_b, blocks_a, blocks_b, scaled, squares, rates, group_out, hidden,
     out_0, in_0, sums_0, own_0, combined_0, landed_0,
     out_1, in_1, sums_1, own_1, combined_1, landed_1, total_1,
     out_2, in_2, sums_2, own_2, combined_2, landed_2,
-    fetched, sems,
+    tally, fetched, sems,
 ):
     place = Place()
     x, core, y, z = place.x, place.core, place.y, place.z
@@ -193,8 +186,8 @@
         pltpu.make_async_copy(src, dst, fetched.at[i])
         for i, (src, dst) in enumerate((
             (stream, blocks_a.at[mine]),
-            (w_in, mixer.at[z, y, pl.ds(0, 128), :]),
-            (w_out, mixer.at[z, y, pl.ds(128, 128), :]),
+            (w_in, mixer_in.at[z, y]),
+            (w_out, mixer_out.at[z, y]),
             (w_gate, gate_in),
             (w_up, up_in),
             (w_down, down_in),
@@ -213,13 +206,14 @@
     def fresh():
         return sems.at[next(taken)]
 
-    gathers = [Gather(place, fresh, buf) for buf in (mixer, pair_a, pair_b, down_a, down_b)]
-    g_mix, g_a, g_b, g_da, g_db = gathers
+    sent = fresh()
+    gathers = [Gather(place, fresh, sent, buf) for buf in (mixer_in, mixer_out, pair_a, pair_b, down_a, down_b)]
+    g_in, g_out, g_a, g_b, g_da, g_db = gathers
     streams = (0, 1)
     rows_each = tokens // 2
     half = rows_each // 2
-    s_in = [Spread(place, fresh, blocks_a, rows_each * t, rows_each) for t in streams]
-    s_mid = [Spread(place, fresh, blocks_b, rows_each * t, rows_each) for t in streams]
+    s_in = [Spread(place, fresh, sent, blocks_a, rows_each * t, rows_each) for t in streams]
+    s_mid = [Spread(place, fresh, sent, blocks_b, rows_each * t, rows_each) for t in streams]
 
     def take(spread, gain_ref, step, other=False, first=False):
         index = spread.index(step, other)
@@ -249,43 +243,49 @@
         steps = (2, 1, 3, 0)
 
         def __init__(self, t, *buffers):
-            super().__init__(place, fresh)
+            super().__init__(place, fresh, sent)
             self.out, self.into, self.sums, self.own, self.combined, self.landed = (
                 buffer.at[t] for buffer in buffers
             )
-            self.sent_pair, self.sent, self.pair_0, self.pair_1, self.got_far, self.got = (
-                fresh() for _ in range(6)
+            self.pair_0, self.pair_1, self.got_far, self.got = (
+                fresh() for _ in range(4)
             )
 
-        def give(self):
-            for j in range(4):
-                landed = self.pair_1 if j else self.pair_0
-                self.send(self.out.at[j], self.into.at[j], self.sent_pair, landed, "core", 0)
+        def give(self, j):
+            landed = self.pair_1 if j else self.pair_0
+            self.send(self.out.at[j], self.into.at[j], landed, "core", 0)
+
+        def add(self, j):
+            if j == 0:
+                self.wait(self.pair_0, self.into.at[0])
+            if j == 1:
+                self.wait(self.pair_1, self.into.at[pl.ds(1, 3)])
+            total = self.own[j] + self.into[j].astype(F32)
+            if j == 3:
+                self.own[j] = total
+            else:
+                self.sums[j] = total.astype(BF16)
 
         def start(self):
             sums, landed = self.sums, self.landed
-            for j in range(4):
-                if j < 2:
-                    self.wait(*((self.pair_0, self.into.at[0]), (self.pair_1, self.into.at[pl.ds(1, 3)]))[j])
-                total = self.own[j] + self.into[j].astype(F32)
-                if j == 3:
-                    self.own[j] = total
-                else:
-                    sums[j] = total.astype(BF16)
-                if j == 0:
-                    self.send(sums.at[0, rows_of(0)], landed.at[0], self.sent, self.got_far, "x", 1)
-                    self.send(sums.at[0, rows_of(1)], landed.at[1], self.sent, self.got_far, "x", -1)
-                if j == 1:
-                    self.send(sums.at[1, rows_of(1)], landed.at[2], self.sent, self.got, "x", 1)
-                if j == 2:
-                    self.send(sums.at[2, rows_of(0)], landed.at[3], self.sent, self.got, "x", -1)
+            self.add(0)
+            self.send(sums.at[0, rows_of(0)], landed.at[0], self.got_far, "x", 1)
+            self.send(sums.at[0, rows_of(1)], landed.at[1], self.got_far, "x", -1)
+
+        def start_near(self):
+            sums, landed = self.sums, self.landed
+            self.add(1)
+            self.send(sums.at[1, rows_of(1)], landed.at[2], self.got, "x", 1)
+            self.add(2)
+            self.send(sums.at[2, rows_of(0)], landed.at[3], self.got, "x", -1)
+            self.add(3)
 
         def forward(self):
             self.wait(self.got_far, self.landed.at[pl.ds(0, 2)])
             for side, step in ((0, 1), (1, -1)):
                 total = self.sums[1 + side, rows_of(side), :].astype(F32) + self.landed[side].astype(F32)
                 self.combined[side] = total.astype(BF16)
-                self.send(self.combined.at[side], self.landed.at[4 + side], self.sent, self.got, "x", step)
+                self.send(self.combined.at[side], self.landed.at[4 + side], self.got, "x", step)
 
         def result(self, store):
             self.wait(self.got, self.landed.at[pl.ds(2, 4)])
@@ -297,19 +297,31 @@
                     + self.landed[4 + side].astype(F32),
                 )
 
-        def drain(self):
-            self.wait(self.sent_pair, self.out)
-            self.wait(self.sent, self.sums)
 
     def pair_up(sums, products):
-        for group in products.groups:
+        first, rest = products.groups
+
+        def for_other(group):
             for i, j, value in products(group, 1 - core):
                 sums[i].out[j] = value.astype(BF16)
-        for each in sums:
-            each.give()
-        for group in products.groups:
+
+        def for_this(group):
             for i, j, value in products(group, core):
                 sums[i].own[j] = value
+
+        def give(group):
+            for j in group:
+                for each in sums:
+                    each.give(j)
+
+        for_other(first)
+        give(first)
+        for_other(rest)
+        for_this(first)
+        give(rest)
+        for each in sums:
+            each.start()
+        for_this(rest)
 
     r_mix = [Summed(t, out_0, in_0, sums_0, own_0, combined_0, landed_0) for t in streams]
     r_one = [Summed(t, out_1, in_1, sums_1, own_1, combined_1, landed_1) for t in streams]
@@ -320,37 +332,33 @@
 
     reach = jnp.where(x == 0, 2, jnp.where(x == 1, 4, jnp.where(x == 2, 8, 16)))
 
-    def mix(t):
-        first = rows_each * t
-        pooled = jnp.dot(
-            scaled[first : first + rows_each, :], mixer[:, :, 0:128, :].reshape(2048, 128),
-            preferred_element_type=F32,
-        )
-        pooled = (pooled * rates[first : first + rows_each, :]).astype(BF16)
+    def mix():
+        pooled = jnp.dot(scaled[...], mixer_in[...].reshape(2048, 128), preferred_element_type=F32)
+        pooled = (pooled * rates[...]).astype(BF16)
         query = lax.broadcasted_iota(jnp.int32, (SEQ, SEQ), 0)
         earlier = lax.broadcasted_iota(jnp.int32, (SEQ, SEQ), 1)
         inside = jnp.where((earlier <= query) & (earlier > query - reach), 1.0, 0.0).astype(BF16)
         counts = jnp.minimum(query + 1, reach).astype(F32)
         scale = pool_s[...].astype(F32)
-        for s in range(rows_each // SEQ):
-            part = pooled[s * SEQ : s * SEQ + SEQ]
-            window = jnp.dot(inside, part, preferred_element_type=F32)
-            contrast = (window / counts - part.astype(F32)).astype(BF16)
-            mixed = jnp.dot(contrast, pool_w[0], preferred_element_type=F32)
-            group_out[first + s * SEQ : first + s * SEQ + SEQ, :] = (mixed * scale).astype(BF16)
-
-    def mix_products(t):
-        first = rows_each * t
-
-        def products(group, owner_core):
-            for j in group:
-                pair = mixer[(x + Summed.steps[j]) % RING, pl.ds(2 * owner_core, 2), 128:256, :]
-                weights = jnp.concatenate([pair[0], pair[1]], axis=1)
-                tokens_of = group_out[first : first + rows_each, :]
-                yield 0, j, jnp.dot(tokens_of, weights, preferred_element_type=F32)
-
-        products.groups = ((0,), (1,), (2,), (3,))
-        return products
+        sequences = [pooled[s * SEQ : s * SEQ + SEQ] for s in range(tokens // SEQ)]
+        windows = [jnp.dot(inside, part, preferred_element_type=F32) for part in sequences]
+        contrasts = [
+            (window / counts - part.astype(F32)).astype(BF16) for window, part in zip(windows, sequences)
+        ]
+        mixed = jnp.dot(jnp.concatenate(contrasts, axis=0), pool_w[0], preferred_element_type=F32)
+        group_out[...] = (mixed * scale).astype(BF16)
+
+    def mix_products(group, owner_core):
+        columns = []
+        for j in group:
+            pair = mixer_out[(x + Summed.steps[j]) % RING, pl.ds(2 * owner_core, 2)]
+            columns.append(jnp.concatenate([pair[0], pair[1]], axis=1))
+        for i, j in enumerate(group):
+            both = jnp.dot(group_out[...], columns[i], preferred_element_type=F32)
+            for t in streams:
+                yield t, j, both[rows_each * t : rows_each * t + rows_each]
+
+    mix_products.groups = ((0, 1), (2, 3))
 
     def ffn_products(buf):
         def products(group, owner_core):
@@ -369,22 +377,29 @@
         products.groups = ((0, 1), (2, 3))
         return products
 
-    def units(t, buf, at, width, column):
-        weights = buf[:, :, :, at : at + 2 * width].reshape(2048, 2 * width)
-        rows = slice(rows_each * t, rows_each * t + rows_each)
-        acts = jnp.dot(scaled[rows, :], weights, preferred_element_type=F32)
-        rate = rates[rows, 0:width]
-        gate, up = acts[:, :width] * rate, acts[:, width:] * rate
-        hidden[rows, column : column + width] = (gate / (1.0 + jnp.exp(-gate)) * up).astype(BF16)
+    def units(chunks):
+        before = None
+        for chunk in (*chunks, None):
+            acts = None
+            if chunk is not None:
+                t, buf, at, width, column = chunk
+                rows = slice(rows_each * t, rows_each * t + rows_each)
+                weights = buf[:, :, :, at : at + 2 * width].reshape(2048, 2 * width)
+                acts = jnp.dot(scaled[rows, :], weights, preferred_element_type=F32)
+            if before is not None:
+                done, (t, _, _, width, column) = before
+                rows = slice(rows_each * t, rows_each * t + rows_each)
+                rate = rates[rows, 0:width]
+                gate, up = done[:, :width] * rate, done[:, width:] * rate
+                hidden[rows, column : column + width] = (gate / (1.0 + jnp.exp(-gate)) * up).astype(BF16)
+            before = acts, chunk
 
     def units_a(t):
-        for chunk in range(3):
-            units(t, pair_a, 256 * chunk, 128, 128 * chunk)
+        units([(t, pair_a, 256 * i, 128, 128 * i) for i in range(3)])
 
     def units_b(t):
-        for chunk in range(2):
-            units(t, pair_b, 256 * chunk, 128, 384 + 128 * chunk)
-        units(t, pair_b, 512, 64, 640)
+        last = (t, pair_b, 512, 64, 640)
+        units([*((t, pair_b, 256 * i, 128, 384 + 128 * i) for i in range(2)), last])
 
     def middle_of(t):
         def store(side, total):
@@ -411,11 +426,16 @@
 
         return store
 
+    def down_relay():
+        g_da.p2_forward()
+        g_db.p2_second()
+
     fetches[0].wait()
     s_in[0].start()
     fetches[1].wait()
     fetches[2].wait()
-    g_mix.p1_own()
+    g_in.p1_own()
+    g_out.p1_own()
     s_in[1].start()
     fetches[3].wait()
     fetches[4].wait()
@@ -436,7 +456,8 @@
     g_b.p1_own()
     for t in streams:
         take(s_in[t], mix_gain, 0, first=True)
-    g_mix.p1_forward()
+    g_in.p1_forward()
+    g_out.p1_forward()
     g_da.p1_own()
     g_db.p1_own()
     s_in[0].forward()
@@ -444,23 +465,23 @@
     for t in streams:
         s_in[t].other_own()
         take(s_in[t], mix_gain, 0, other=True)
-    g_mix.p2_own()
-    g_b.p1_forward()
     s_in[0].near()
     s_in[1].forward()
     for step in (3, 1):
         take(s_in[0], mix_gain, step)
+    g_in.p2_own()
+    g_out.p2_own()
+    g_b.p1_forward()
     s_in[1].near()
-    g_mix.p2_forward()
+    for step in (3, 1):
+        take(s_in[1], mix_gain, step)
+    s_in[0].far()
+    take(s_in[0], mix_gain, 2)
+    s_in[1].far()
+    take(s_in[1], mix_gain, 2)
+    g_in.p2_forward()
     g_da.p1_forward()
     g_db.p1_forward()
-    s_in[0].far()
-    take(s_in[0], mix_gain, 2)
-    for step in (3, 1):
-        take(s_in[1], mix_gain, step)
-    s_in[1].far()
-    take(s_in[1], mix_gain, 2)
-    g_a.p2_own()
     for t in streams:
         s_in[t].other_near()
         take(s_in[t], mix_gain, 3, other=True)
@@ -468,20 +489,21 @@
         s_in[t].other_far()
         take(s_in[t], mix_gain, 2, other=True)
         row_rates(t)
+    g_out.p2_forward()
+    g_a.p2_own()
+    g_in.finish()
+    mix()
+    g_out.finish()
+    pair_up(r_mix, mix_products)
+    r_mix[0].start_near()
+    r_mix[1].start_near()
     g_b.p2_own()
-    g_mix.finish()
-    mix(0)
-    pair_up([r_mix[0]], mix_products(0))
-    mix(1)
-    r_mix[0].start()
-    pair_up([r_mix[1]], mix_products(1))
-    r_mix[1].start()
     r_mix[0].forward()
     r_mix[1].forward()
+    g_a.p2_forward()
     r_mix[0].result(middle_of(0))
     s_mid[0].start()
     take(s_mid[0], ffn_gain, 0, first=True)
-    g_a.p2_forward()
     g_b.p2_forward()
     r_mix[1].result(middle_of(1))
     s_mid[1].start()
@@ -512,8 +534,7 @@
         row_rates(t)
     g_a.finish()
     units_a(0)
-    g_da.p2_forward()
-    g_db.p2_second()
+    down_relay()
     units_a(1)
     g_b.finish()
     units_b(0)
@@ -522,22 +543,21 @@
     g_da.finish()
     pair_up(r_one, ffn_products(down_a))
     for t in streams:
-        r_one[t].start()
+        r_one[t].start_near()
     g_db.finish()
     pair_up(r_two, ffn_products(down_b))
     for t in streams:
         r_one[t].forward()
     for t in streams:
-        r_two[t].start()
+        r_two[t].start_near()
+    for t in streams:
+        r_two[t].forward()
     for t in streams:
         r_one[t].result(first_of(t))
     for t in streams:
-        r_two[t].forward()
-    for t in streams:
         r_two[t].result(result_of(t))
 
-    for net in [*gathers, *s_in, *s_mid, *r_mix, *r_one, *r_two]:
-        net.drain()
+    pltpu.make_async_copy(tally, tally, sent).wait()
 
 
 def summing(tokens, width):
@@ -550,6 +570,11 @@
         pltpu.VMEM((2, 2, rows // 2, width), BF16),
         pltpu.VMEM((2, 6, rows // 2, width), BF16),
     ]
+
+
+def sent_rows(tokens):
+    weights = 128 + 128 + 128 * 6 + 128 * 5 + 352 + 352
+    return 15 * weights + 7 * tokens * 2 * (2 + 1) + 7 * tokens * 2
 
 
 def on_device(stream, in_weight, pool_weight, pool_scale, out_weight, mix_gain, ffn_gain, gate_weight, up_weight, down_weight):
@@ -568,7 +593,8 @@
             pltpu.VMEM((704, 128), BF16),
             pltpu.VMEM((1, 128, 128), BF16),
             pltpu.VMEM((1, 128), BF16),
-            pltpu.VMEM((4, 4, 256, 128), BF16),
+            pltpu.VMEM((4, 4, 128, 128), BF16),
+            pltpu.VMEM((4, 4, 128, 128), BF16),
             pltpu.VMEM((4, 4, 128, 768), BF16),
             pltpu.VMEM((4, 4, 128, 640), BF16),
             pltpu.VMEM((4, 4, 352, 128), BF16),
@@ -584,11 +610,12 @@
             *summing(tokens, 128),
             pltpu.VMEM((tokens, 128), F32),
             *summing(tokens, 128),
+            pltpu.VMEM((sent_rows(tokens), 128), BF16),
             pltpu.SemaphoreType.DMA((10,)),
-            pltpu.SemaphoreType.DMA((94,)),
+            pltpu.SemaphoreType.DMA((73,)),
         ],
         compiler_params=pltpu.CompilerParams(
-            collective_id=0, has_side_effects=True, vmem_limit_bytes=40 * 1024 * 1024
+            collective_id=0, has_side_effects=True, vmem_limit_bytes=48 * 1024 * 1024
         ),
     )(*(pltpu.with_memory_space_constraint(a, pltpu.HBM) for a in (
         stream, in_weight, pool_weight, pool_scale.reshape(1, -1), out_weight,

time: 72.5 us -> 72.3 us (level)
  no operation moved by 1% of the time
where the time goes in v4:
time: 72.3 us; the launch traced here: 72.2 us
  Pallas kernels  71.5 us (99%)
    pallas_call x1, Pallas kernels, on_device(): pl.pallas_call(kernel, out_shape=jax.ShapeDtypeStruct(stream.shape, BF16)...  71.5 us

profile of v4, /device:TPU:1, one launch (start us, length us, event | category | flops | bytes accessed | tf_op | source)
XLA Modules:
  0.0 72.2 jit_solution(9362778706367499644)
XLA Ops:
  0.0 71.5 %shard_map.100 = bf16[512,256]{1,0:T(8,128)(2,1)S(1)} custom-call(bf16[512,256]{1,0:T(8,128)(2,1)} %stream.1, bf16[128,128]{1,0:T(8,128)(2,1)} %w_in.1, bf16[1,128,128]{2,1,0:T(8,128)(2,1)} %pool_w_in.1, bf16[1,128]{1,0:T(2,128)(2,1)} %bitcast.9, bf16[128,128]{1,0:T(8,128)(2,1)} %w_out.1, bf16[16,128]{1,0:T(8,128)(2,1)} %bitcast.7, bf16[16,128]{1,0:T(8,128)(2,1)} %bitcast.8, ...), custom_call_target="tpu_custom_call" | custom-call | tf_op jit(solution)/shard_map/pallas_call | solution.py:582
  71.5 0.7 copy.12

commit v5 on v4

--- a/solution.py
+++ b/solution.py
@@ -358,7 +358,7 @@
             for t in streams:
                 yield t, j, both[rows_each * t : rows_each * t + rows_each]
 
-    mix_products.groups = ((0, 1), (2, 3))
+    mix_products.groups = ((0,), (1, 2, 3))
 
     def ffn_products(buf):
         def products(group, owner_core):
@@ -374,7 +374,7 @@
                 for i, j in enumerate(group):
                     yield t, j, both[rows_each * t : rows_each * t + rows_each, 128 * i : 128 * i + 128]
 
-        products.groups = ((0, 1), (2, 3))
+        products.groups = ((0,), (1, 2, 3))
         return products
 
     def units(chunks):

time: 72.3 us -> 71.9 us (level)
  no operation moved by 1% of the time
where the time goes in v5:
time: 71.9 us; the launch traced here: 71.8 us
  Pallas kernels  71.1 us (99%)
    pallas_call x1, Pallas kernels, on_device(): pl.pallas_call(kernel, out_shape=jax.ShapeDtypeStruct(stream.shape, BF16)...  71.1 us

profile of v5, /device:TPU:1, one launch (start us, length us, event | category | flops | bytes accessed | tf_op | source)
XLA Modules:
  0.0 71.8 jit_solution(17999191720127199727)
XLA Ops:
  0.0 71.1 %shard_map.100 = bf16[512,256]{1,0:T(8,128)(2,1)S(1)} custom-call(bf16[512,256]{1,0:T(8,128)(2,1)} %stream.1, bf16[128,128]{1,0:T(8,128)(2,1)} %w_in.1, bf16[1,128,128]{2,1,0:T(8,128)(2,1)} %pool_w_in.1, bf16[1,128]{1,0:T(2,128)(2,1)} %bitcast.9, bf16[128,128]{1,0:T(8,128)(2,1)} %w_out.1, bf16[16,128]{1,0:T(8,128)(2,1)} %bitcast.7, bf16[16,128]{1,0:T(8,128)(2,1)} %bitcast.8, ...), custom_call_target="tpu_custom_call" | custom-call | tf_op jit(solution)/shard_map/pallas_call | solution.py:582
  71.1 0.7 copy.12

commit v6 on v5

--- a/solution.py
+++ b/solution.py
@@ -113,9 +113,8 @@
     def __init__(self, place, fresh, sent, buf, first, rows):
         super().__init__(place, fresh, sent)
         self.buf, self.first, self.rows = buf, first, rows
-        self.got_0, self.got_1, self.got_2, self.pair_0, self.pair_1, self.pair_2 = (
-            fresh() for _ in range(6)
-        )
+        self.semaphores = [fresh() for _ in range(6)]
+        self.got_0, self.got_1, self.got_2, self.pair_0, self.pair_1, self.pair_2 = self.semaphores
 
     def index(self, step, other=False):
         core = 1 - self.place.core if other else self.place.core
@@ -206,6 +205,10 @@
     def fresh():
         return sems.at[next(taken)]
 
+    def again(nets):
+        used = iter([semaphore for net in nets for semaphore in net.semaphores])
+        return lambda: next(used)
+
     sent = fresh()
     gathers = [Gather(place, fresh, sent, buf) for buf in (mixer_in, mixer_out, pair_a, pair_b, down_a, down_b)]
     g_in, g_out, g_a, g_b, g_da, g_db = gathers
@@ -213,7 +216,8 @@
     rows_each = tokens // 2
     half = rows_each // 2
     s_in = [Spread(place, fresh, sent, blocks_a, rows_each * t, rows_each) for t in streams]
-    s_mid = [Spread(place, fresh, sent, blocks_b, rows_each * t, rows_each) for t in streams]
+    old = again(s_in)
+    s_mid = [Spread(place, old, sent, blocks_b, rows_each * t, rows_each) for t in streams]
 
     def take(spread, gain_ref, step, other=False, first=False):
         index = spread.index(step, other)
@@ -242,14 +246,13 @@
     class Summed(Net):
         steps = (2, 1, 3, 0)
 
-        def __init__(self, t, *buffers):
+        def __init__(self, fresh, t, *buffers):
             super().__init__(place, fresh, sent)
             self.out, self.into, self.sums, self.own, self.combined, self.landed = (
                 buffer.at[t] for buffer in buffers
             )
-            self.pair_0, self.pair_1, self.got_far, self.got = (
-                fresh() for _ in range(4)
-            )
+            self.semaphores = [fresh() for _ in range(4)]
+            self.pair_0, self.pair_1, self.got_far, self.got = self.semaphores
 
         def give(self, j):
             landed = self.pair_1 if j else self.pair_0
@@ -323,9 +326,10 @@
             each.start()
         for_this(rest)
 
-    r_mix = [Summed(t, out_0, in_0, sums_0, own_0, combined_0, landed_0) for t in streams]
-    r_one = [Summed(t, out_1, in_1, sums_1, own_1, combined_1, landed_1) for t in streams]
-    r_two = [Summed(t, out_2, in_2, sums_2, own_2, combined_2, landed_2) for t in streams]
+    r_mix = [Summed(fresh, t, out_0, in_0, sums_0, own_0, combined_0, landed_0) for t in streams]
+    old = again(r_mix)
+    r_one = [Summed(old, t, out_1, in_1, sums_1, own_1, combined_1, landed_1) for t in streams]
+    r_two = [Summed(fresh, t, out_2, in_2, sums_2, own_2, combined_2, landed_2) for t in streams]
 
     def token_rows(t, side):
         return pl.ds(rows_each * t + half * side, half)
@@ -612,7 +616,7 @@
             *summing(tokens, 128),
             pltpu.VMEM((sent_rows(tokens), 128), BF16),
             pltpu.SemaphoreType.DMA((10,)),
-            pltpu.SemaphoreType.DMA((73,)),
+            pltpu.SemaphoreType.DMA((53,)),
         ],
         compiler_params=pltpu.CompilerParams(
             collective_id=0, has_side_effects=True, vmem_limit_bytes=48 * 1024 * 1024

time: 71.9 us -> 71.7 us (level)
  no operation moved by 1% of the time
where the time goes in v6:
time: 71.7 us; the launch traced here: 71.6 us
  Pallas kernels  70.9 us (99%)
    pallas_call x1, Pallas kernels, on_device(): pl.pallas_call(kernel, out_shape=jax.ShapeDtypeStruct(stream.shape, BF16)...  70.9 us

profile of v6, /device:TPU:1, one launch (start us, length us, event | category | flops | bytes accessed | tf_op | source)
XLA Modules:
  0.0 71.6 jit_solution(3323724886753479592)
XLA Ops:
  0.0 70.9 %shard_map.100 = bf16[512,256]{1,0:T(8,128)(2,1)S(1)} custom-call(bf16[512,256]{1,0:T(8,128)(2,1)} %stream.1, bf16[128,128]{1,0:T(8,128)(2,1)} %w_in.1, bf16[1,128,128]{2,1,0:T(8,128)(2,1)} %pool_w_in.1, bf16[1,128]{1,0:T(2,128)(2,1)} %bitcast.9, bf16[128,128]{1,0:T(8,128)(2,1)} %w_out.1, bf16[16,128]{1,0:T(8,128)(2,1)} %bitcast.7, bf16[16,128]{1,0:T(8,128)(2,1)} %bitcast.8, ...), custom_call_target="tpu_custom_call" | custom-call | tf_op jit(solution)/shard_map/pallas_call | solution.py:586
  70.9 0.7 copy.12

commit v7 on v5

--- a/solution.py
+++ b/solution.py
@@ -180,8 +180,6 @@
 
     barrier = pltpu.get_barrier_semaphore()
     neighbours = [place.to(a, s) for a in "xyz" for s in (1, -1)] + [place.to("core", 0)]
-    for device in neighbours:
-        pl.semaphore_signal(barrier, inc=1, device_id=device, device_id_type=pl.DeviceIdType.MESH)
     fetches = [
         pltpu.make_async_copy(src, dst, fetched.at[i])
         for i, (src, dst) in enumerate((
@@ -197,8 +195,10 @@
             (pool_s_in, pool_s),
         ))
     ]
-    for fetch in fetches:
-        fetch.start()
+    for i in (1, 2, 3, 4, 0, 5, 6, 7, 8, 9):
+        fetches[i].start()
+    for device in neighbours:
+        pl.semaphore_signal(barrier, inc=1, device_id=device, device_id_type=pl.DeviceIdType.MESH)
     pl.semaphore_wait(barrier, len(neighbours))
 
     taken = iter(range(sems.shape[0]))
@@ -430,13 +430,13 @@
         g_da.p2_forward()
         g_db.p2_second()
 
-    fetches[0].wait()
-    s_in[0].start()
     fetches[1].wait()
     fetches[2].wait()
     g_in.p1_own()
     g_out.p1_own()
-    s_in[1].start()
+    fetches[0].wait()
+    for t in streams:
+        s_in[t].start()
     fetches[3].wait()
     fetches[4].wait()
     for tile in range(5):

time: 71.9 us -> 71.9 us (level)
  no operation moved by 1% of the time
where the time goes in v7:
time: 71.9 us
  Pallas kernels  71.1 us (99%)
    pallas_call x1, Pallas kernels, on_device(): pl.pallas_call(kernel, out_shape=jax.ShapeDtypeStruct(stream.shape, BF16)...  71.1 us

profile of v7, /device:TPU:1, one launch (start us, length us, event | category | flops | bytes accessed | tf_op | source)
XLA Modules:
  0.0 71.9 jit_solution(1014856213114625203)
XLA Ops:
  0.0 71.1 %shard_map.100 = bf16[512,256]{1,0:T(8,128)(2,1)S(1)} custom-call(bf16[512,256]{1,0:T(8,128)(2,1)} %stream.1, bf16[128,128]{1,0:T(8,128)(2,1)} %w_in.1, bf16[1,128,128]{2,1,0:T(8,128)(2,1)} %pool_w_in.1, bf16[1,128]{1,0:T(2,128)(2,1)} %bitcast.9, bf16[128,128]{1,0:T(8,128)(2,1)} %w_out.1, bf16[16,128]{1,0:T(8,128)(2,1)} %bitcast.7, bf16[16,128]{1,0:T(8,128)(2,1)} %bitcast.8, ...), custom_call_target="tpu_custom_call" | custom-call | tf_op jit(solution)/shard_map/pallas_call | solution.py:582
  71.1 0.7 copy.12

commit v8 on v5

--- a/solution.py
+++ b/solution.py
@@ -298,7 +298,7 @@
                 )
 
 
-    def pair_up(sums, products):
+    def pair_up(sums, products, earlier=()):
         first, rest = products.groups
 
         def for_other(group):
@@ -321,6 +321,8 @@
         give(rest)
         for each in sums:
             each.start()
+        for each in earlier:
+            each.forward()
         for_this(rest)
 
     r_mix = [Summed(t, out_0, in_0, sums_0, own_0, combined_0, landed_0) for t in streams]
@@ -545,9 +547,7 @@
     for t in streams:
         r_one[t].start_near()
     g_db.finish()
-    pair_up(r_two, ffn_products(down_b))
-    for t in streams:
-        r_one[t].forward()
+    pair_up(r_two, ffn_products(down_b), r_one)
     for t in streams:
         r_two[t].start_near()
     for t in streams:

time: 71.9 us -> 71.9 us (level)
  no operation moved by 1% of the time
where the time goes in v8:
time: 71.9 us; the launch traced here: 71.8 us
  Pallas kernels  71.1 us (99%)
    pallas_call x1, Pallas kernels, on_device(): pl.pallas_call(kernel, out_shape=jax.ShapeDtypeStruct(stream.shape, BF16)...  71.1 us

profile of v8, /device:TPU:1, one launch (start us, length us, event | category | flops | bytes accessed | tf_op | source)
XLA Modules:
  0.0 71.8 jit_solution(8696816443705269527)
XLA Ops:
  0.0 71.1 %shard_map.100 = bf16[512,256]{1,0:T(8,128)(2,1)S(1)} custom-call(bf16[512,256]{1,0:T(8,128)(2,1)} %stream.1, bf16[128,128]{1,0:T(8,128)(2,1)} %w_in.1, bf16[1,128,128]{2,1,0:T(8,128)(2,1)} %pool_w_in.1, bf16[1,128]{1,0:T(2,128)(2,1)} %bitcast.9, bf16[128,128]{1,0:T(8,128)(2,1)} %w_out.1, bf16[16,128]{1,0:T(8,128)(2,1)} %bitcast.7, bf16[16,128]{1,0:T(8,128)(2,1)} %bitcast.8, ...), custom_call_target="tpu_custom_call" | custom-call | tf_op jit(solution)/shard_map/pallas_call | solution.py:582
  71.1 0.7 copy.12
